TPU v7x, 128 devices: a whole 4x4x4 slice. The times are simulated.
128 devices in a mesh: sp: 32 (over z, y, core), tp: 4 (over x).
Axes of the slice: x: 4, y: 4, z: 4, core: 2. Of those that a mesh axis runs over, the one named last changes fastest.
Arguments:
- queries: bfloat16 [16384, 1024], P('sp', 'tp'), may hold values from -6 to 6
- key_heads: bfloat16 [16384, 512], P('sp', 'tp'), may hold values from -6 to 6
- value_heads: bfloat16 [16384, 512], P('sp', 'tp'), may hold values from -70 to 70
- documents: int32 [16384], P('sp'), may hold values from 0 to 8, never falling along the last dimension, each value on 1 to 10240 neighbouring positions
- query_gain: float32 [128], replicated, may hold values from 0.1 to 8
- key_gain: float32 [128], replicated, may hold values from 0.1 to 8
- out_gain: float32 [1024], replicated, may hold values from 0.1 to 1.9
- out_proj: bfloat16 [1024, 2048], replicated, may hold values from -0.1875 to 0.1875
- residual: bfloat16 [16384, 2048], P(('sp', 'tp')), may hold values from -6 to 6
- mid_gain: float32 [2048], replicated, may hold values from 0.1 to 1.9
- mid_bias: float32 [2048], replicated, may hold values from -1.5 to 1.5
- routes: int32 [16384, 2], P(('sp', 'tp')), may hold values from 0 to 127, all different within a row; in each aligned block of 128 rows (0 to 127, 128 to 255, ...) at most 4 rows name the same one
- route_weights: float32 [16384, 2], P(('sp', 'tp')), may hold values from 0.2 to 2
- expert_gate: bfloat16 [128, 2048, 512], P(('sp', 'tp')), may hold values from -0.125 to 0.125
- expert_up: bfloat16 [128, 2048, 512], P(('sp', 'tp')), may hold values from -0.125 to 0.125
- expert_down: bfloat16 [128, 512, 2048], P(('sp', 'tp')), may hold values from -0.25 to 0.25
- final_gain: float32 [2048], replicated, may hold values from 0.1 to 1.9
- final_bias: float32 [2048], replicated, may hold values from -1.5 to 1.5
Outputs:
- layer_out: bfloat16 [16384, 2048], P(('sp', 'tp'))
Inputs may be any that keep to these rules, and one draw needn't show every extreme that they name: `documents`: never falls along the sequence; each document holds 1 to 10240 positions and one holds exactly 10240. `routes`: each row names 2 different experts; among the rows of one device (aligned blocks of 128 rows) no expert is named more than 4 times, and exactly 4 times in some block.
All inputs are finite; a program needn't handle non-finite values.
Results may differ from a plain program's by a relative error of at most 0.014.
The roundings to bfloat16 on the way count: a program that leaves them out, or rounds other values in their place, can miss the bound.
Values may be sent and summed in bfloat16 or wider, within the bound.
A program may use at most 128 MiB of HBM per device.

v0:
```python
import math

import jax
import jax.numpy as jnp
from jax import lax
from jax.sharding import PartitionSpec as P

HEAD = 128
GRID = 64


eps_norm = 1e-06
alpha_mix = 8.0**0.25
theta_base = 10000.0


def sent_together(arrays, axis, dim, along):
    widths = [a.shape[along] for a in arrays]
    both = jnp.concatenate(arrays, axis=along)
    filled = lax.all_gather(both, axis, axis=dim, tiled=True)
    return tuple(jnp.split(filled, [sum(widths[:k]) for k in range(1, len(widths))], axis=along))


def split_up(shard, dim, length):
    before, after = (shard.shape[:dim], shard.shape[dim + 1 :])
    return jnp.moveaxis(shard.reshape(*before, length, -1, *after), dim, 0)


def sent_and_summed(shard, axis, dim):
    tiles = split_up(shard, dim, lax.axis_size(axis))
    arrived = lax.all_to_all(tiles, axis, split_axis=0, concat_axis=0, tiled=True)
    return arrived.sum(axis=0)


def rotary_tables(row_total, offset):
    positions = offset + jnp.arange(row_total, dtype=jnp.int32)
    grid_row = (positions // GRID).astype(jnp.float32)
    grid_col = (positions % GRID).astype(jnp.float32)
    pair_count = HEAD // 4
    inv_freq = theta_base ** (-jnp.arange(pair_count, dtype=jnp.float32) / pair_count)
    angles = jnp.concatenate(
        [grid_row[:, None] * inv_freq[None, :], grid_col[:, None] * inv_freq[None, :]], axis=1
    )
    return (jnp.cos(angles), jnp.sin(angles))


def normed_rotated(heads_in, gain_vec, cosine_table, sine_table):
    values = heads_in.astype(jnp.float32)
    inv_rms = lax.rsqrt(jnp.mean(values * values, axis=-1, keepdims=True) + eps_norm)
    values = values * inv_rms * gain_vec
    half_dim = HEAD // 2
    first_half = values[..., :half_dim]
    second_half = values[..., half_dim:]
    cosine_part = cosine_table[:, None, :]
    sine_part = sine_table[:, None, :]
    turned = jnp.concatenate(
        [
            first_half * cosine_part - second_half * sine_part,
            second_half * cosine_part + first_half * sine_part,
        ],
        axis=-1,
    )
    return turned.astype(jnp.bfloat16)


def layer_norm(stream, gain_vec, bias_vec):
    center = jnp.mean(stream, axis=-1, keepdims=True)
    spread = jnp.mean(jnp.square(stream - center), axis=-1, keepdims=True)
    return (stream - center) * lax.rsqrt(spread + eps_norm) * gain_vec + bias_vec


def per_device(
    queries,
    key_heads,
    value_heads,
    documents,
    query_gain,
    key_gain,
    out_gain,
    out_proj,
    residual,
    mid_gain,
    mid_bias,
    routes,
    route_weights,
    expert_gate,
    expert_up,
    expert_down,
    final_gain,
    final_bias,
):
    tok_rows = queries.shape[0]
    query_local = queries.shape[1] // HEAD
    key_local = key_heads.shape[1] // HEAD
    grouped = query_local // key_local
    offset = lax.axis_index("sp") * tok_rows
    cosine_table, sine_table = rotary_tables(tok_rows, offset)
    query_rot = normed_rotated(
        queries.reshape(tok_rows, query_local, HEAD), query_gain, cosine_table, sine_table
    ).reshape(tok_rows, key_local, grouped, HEAD)
    key_rot = normed_rotated(
        key_heads.reshape(tok_rows, key_local, HEAD), key_gain, cosine_table, sine_table
    ).reshape(tok_rows, key_local * HEAD)
    first_doc = documents[0]
    last_doc = documents[tok_rows - 1]
    start_state = (
        jnp.full((key_local, grouped, tok_rows), -1e30, jnp.float32),
        jnp.zeros((key_local, grouped, tok_rows), jnp.float32),
        jnp.zeros((key_local, grouped, tok_rows, HEAD), jnp.float32),
    )
    key_part, value_part, doc_part = (
        *sent_together((key_rot, value_heads), "sp", 0, 1),
        lax.all_gather(documents, "sp", axis=0, tiled=True),
    )
    piece_rows = key_part.shape[0]
    block_rows = math.gcd(piece_rows, 512)
    block_count = piece_rows // block_rows
    blocks = (
        key_part.reshape(block_count, block_rows, key_local, HEAD),
        value_part.reshape(block_count, block_rows, key_local, HEAD),
        doc_part.reshape(block_count, block_rows),
    )

    def advance(running, block_set):
        key_block, value_block, doc_block = block_set
        running_max, running_total, running_sum = running
        scores = jnp.einsum(
            "qkgd,tkd->kgqt", query_rot, key_block, preferred_element_type=jnp.float32
        ) * HEAD ** (-0.5)
        allowed = (documents[:, None] == doc_block[None, :])[None, None]
        scores = jnp.where(allowed, scores, -1e30)
        new_max = jnp.maximum(running_max, jnp.max(scores, axis=-1))
        weights = jnp.where(allowed, jnp.exp(scores - new_max[..., None]), 0.0)
        rescale = jnp.exp(running_max - new_max)
        new_total = running_total * rescale + jnp.sum(weights, axis=-1)
        new_sum = running_sum * rescale[..., None] + jnp.einsum(
            "kgqt,tkd->kgqd",
            weights.astype(jnp.bfloat16),
            value_block,
            preferred_element_type=jnp.float32,
        )
        return ((new_max, new_total, new_sum), None)

    def process(running):
        result, unused = lax.scan(advance, running, blocks)
        return result

    touches = (doc_part[0] <= last_doc) & (doc_part[piece_rows - 1] >= first_doc)
    final_max, final_total, final_sum = lax.cond(
        touches, process, lambda running: running, start_state
    )
    attention = jnp.transpose(final_sum / final_total[..., None], (2, 0, 1, 3))
    attention = attention.reshape(tok_rows, query_local * HEAD).astype(jnp.bfloat16)
    local_width = query_local * HEAD
    attn_float = attention.astype(jnp.float32)
    squares = sent_and_summed(jnp.sum(attn_float * attn_float, axis=1), "tp", 0)
    mean_square = squares / out_gain.shape[0]
    own_gain = lax.dynamic_slice_in_dim(
        out_gain, lax.axis_index("tp") * local_width, local_width, 0
    )
    own_rows = lax.dynamic_slice_in_dim(
        out_proj, lax.axis_index("tp") * local_width, local_width, 0
    )
    scaled = (attn_float * own_gain).astype(jnp.bfloat16)
    projected = lax.psum_scatter(
        jnp.dot(scaled, own_rows, preferred_element_type=jnp.float32).astype(jnp.bfloat16),
        "tp",
        scatter_dimension=0,
        tiled=True,
    ).astype(jnp.float32)
    projected = projected * lax.rsqrt(mean_square + eps_norm)[:, None]
    middle = layer_norm(
        alpha_mix * residual.astype(jnp.float32) + projected, mid_gain, mid_bias
    ).astype(jnp.bfloat16)
    out_rows = middle.shape[0]
    model_width = middle.shape[1]
    top_count = routes.shape[1]
    local_experts = expert_gate.shape[0]
    sp_size = lax.axis_size("sp")
    tp_size = lax.axis_size("tp")
    expert_total = local_experts * sp_size * tp_size
    capacity = 2 * out_rows * top_count // expert_total
    flat_routes = routes.reshape(-1)
    one_hot = (flat_routes[:, None] == jnp.arange(expert_total, dtype=jnp.int32)[None, :]).astype(
        jnp.int32
    )
    rank_in = jnp.sum((jnp.cumsum(one_hot, axis=0) - one_hot) * one_hot, axis=1)
    target = flat_routes * capacity + rank_in
    outbound = (
        jnp.zeros((expert_total * capacity, model_width), jnp.bfloat16)
        .at[target]
        .set(jnp.repeat(middle, top_count, axis=0))
    )
    arrived = lax.all_to_all(
        outbound.reshape(expert_total, capacity, model_width),
        ("sp", "tp"),
        split_axis=0,
        concat_axis=0,
        tiled=True,
    )
    item_count = arrived.shape[-2]
    grouped_rows = arrived.reshape(-1, local_experts, item_count, model_width)
    gate_part = jnp.einsum(
        "sekd,edf->sekf", grouped_rows, expert_gate, preferred_element_type=jnp.float32
    )
    up_part = jnp.einsum(
        "sekd,edf->sekf", grouped_rows, expert_up, preferred_element_type=jnp.float32
    )
    hidden = (jax.nn.silu(gate_part) * up_part).astype(jnp.bfloat16)
    served = jnp.einsum("sekf,efd->sekd", hidden, expert_down, preferred_element_type=jnp.float32)
    returned = lax.all_to_all(
        served.astype(jnp.bfloat16).reshape(arrived.shape),
        ("sp", "tp"),
        split_axis=0,
        concat_axis=0,
        tiled=True,
    )
    picked = returned.reshape(expert_total * capacity, model_width)[target]
    picked = picked.astype(jnp.float32).reshape(out_rows, top_count, model_width)
    routed = jnp.sum(picked * route_weights[:, :, None], axis=1)
    return layer_norm(
        alpha_mix * middle.astype(jnp.float32) + routed, final_gain, final_bias
    ).astype(jnp.bfloat16)


def solution(mesh):
    return jax.shard_map(
        per_device,
        mesh=mesh,
        in_specs=(
            P("sp", "tp"),
            P("sp", "tp"),
            P("sp", "tp"),
            P("sp"),
            P(),
            P(),
            P(),
            P(),
            P(("sp", "tp"), None),
            P(),
            P(),
            P(("sp", "tp"), None),
            P(("sp", "tp"), None),
            P(("sp", "tp"), None, None),
            P(("sp", "tp"), None, None),
            P(("sp", "tp"), None, None),
            P(),
            P(),
        ),
        out_specs=P(("sp", "tp"), None),
        check_vma=False,
    )
```

profile of v0, /device:TPU:1, one launch (start us, length us, event | category | flops | bytes accessed | tf_op | source)
XLA Modules:
  0.0 485.2 jit_solution(16943709737238043858)
XLA Ops:
  10.6 27.1 %all-gather = s32[32,1,512]{2,1,0:T(1,128)S(1)} all-gather(s32[1,1,512]{2,1,0:T(1,128)S(1)} %bitcast.177), channel_id=1, replica_groups=mesh['sp'=32,'tp'=4] {'sp'}, dimensions={0}, use_global_device_ids=true | all-gather | bytes 67584 | tf_op jit(solution)/shard_map/all_gather | solution.py:113
  42.7 24.3 %all-gather.3.cloned.1.call-done = bf16[16384,256]{1,0:T(8,128)(2,1)} async-done(((bf16[512,256]{1,0:T(8,128)(2,1)}), bf16[16384,256]{1,0:T(8,128)(2,1)}) %all-gather.3.cloned.1.call-update) | async-done | bytes 8388624 | tf_op jit(solution)/shard_map/all_gather | solution.py:20
  67.0 251.5 %conditional.1 = (f32[1,2,512]{2,1,0:T(2,128)}, f32[1,2,512,128]{2,3,1,0:T(8,128)S(1)}) conditional(s32[]{:T(128)} %bitcast.4, () %tuple.17, (bf16[16384,256]{1,0:T(8,128)(2,1)}, s32[16384]{0:T(1024)S(1)}, s32[512]{0:T(512)S(1)}, bf16[512,1,2,128]{0,3,2,1:T(8,128)(2,1)S(1)}) %tuple.68), branch_computations={%region_2.3_spmd, %region_3.8_spmd} | conditional | flops 275912704 | bytes 37954852 | solution.py:149
  67.0 5.7 %fusion.95 = (bf16[16384,128]{1,0:T(8,128)(2,1)}, bf16[16384,128]{1,0:T(8,128)(2,1)}) fusion(bf16[16384,256]{1,0:T(8,128)(2,1)} %get-tuple-element.67), kind=kLoop, calls=%fused_computation.131 | loop fusion | bytes 16777216 | tf_op jit(solution)/shard_map/split | solution.py:21
  73.0 243.5 %while.14 = (s32[]{:T(128)}, f32[1,2,512]{2,1,0:T(2,128)S(1)}, f32[1,2,512]{2,1,0:T(2,128)}, f32[1,2,512,128]{3,2,1,0:T(8,128)S(1)}, s32[512]{0:T(512)S(1)}, /*i...) while((s32[]{:T(128)}, f32[1,2,512]{2,1,0:T(2,128)S(1)}, ...), condition=%wide.region_7.7_spmd.clone, body=%wide.region_4.6_spmd.clone.sunk | while | flops 275912704 | bytes 17376408 | solution.py:145
  73.2 2.8 fusion.107
  80.2 2.8 fusion.107
  87.8 2.8 fusion.107
  95.4 2.8 fusion.107
  103.1 2.8 fusion.107
  110.7 2.8 fusion.107
  118.3 2.8 fusion.107
  126.0 2.8 fusion.107
  133.6 2.8 fusion.107
  141.2 2.8 fusion.107
  148.8 2.8 fusion.107
  156.5 2.8 fusion.107
  164.1 2.8 fusion.107
  171.7 2.8 fusion.107
  179.4 2.8 fusion.107
  187.0 2.8 fusion.107
  194.6 2.8 fusion.107
  202.2 2.8 fusion.107
  209.9 2.8 fusion.107
  217.5 2.8 fusion.107
  225.1 2.8 fusion.107
  232.8 2.8 fusion.107
  240.4 2.8 fusion.107
  248.0 2.8 fusion.107
  255.7 2.8 fusion.107
  278.5 2.8 fusion.107
  301.4 2.8 fusion.107
  320.0 3.3 convolution_convert_fusion
  325.3 4.0 all-to-all-start
  329.2 4.1 all-to-all-done
  333.3 18.9 %reduce-scatter.2.cloned.1.call-done = bf16[128,2048]{1,0:T(8,128)(2,1)} async-done(((bf16[512,2048]{1,0:T(8,128)(2,1)}), bf16[128,2048]{1,0:T(8,128)(2,1)}) %reduce-scatter.2.cloned.1.call-update) | async-done | bytes 524304 | tf_op jit(solution)/shard_map/reduce_scatter | solution.py:165
  359.5 4.4 scatter_custom_fusion
  363.9 4.1 reshape.459
  368.0 38.8 %all_to_all.19 = bf16[128,4,2048]{2,1,0:T(4,128)(2,1)S(1)} all-to-all(bf16[128,4,2048]{2,1,0:T(4,128)(2,1)} %reshape.459), channel_id=1, replica_groups=mesh['sp'=32,'tp'=4] {'sp','tp'}, dimensions={0} | all-to-all | bytes 4194304 | tf_op jit(solution)/shard_map/all_to_all | solution.py:194
  408.2 3.4 fusion.30
  411.6 7.5 %convolution_convert_fusion.1 = bf16[128,4,2048]{2,0,1:T(8,128)(2,1)} fusion(bf16[1,512,2048]{2,1,0:T(8,128)(2,1)S(1)} %copy-done, bf16[1,2048,512]{2,1,0:T(8,128)(2,1)} %param.36, bf16[128,4,2048]{2,1,0:T(4,128)(2,1)} %copy-done.4, f32[128,1,4,512]{3,0,2,1:T(8,128)} %fusion.30), kind=kOutput, calls=%fused_computation.36 | convolution fusion | flops 2150105088 | bytes 9437184 | tf_op jit(solution)/shard_map/sekf,efd->sekd/dot_general | solution.py:210
  419.1 4.5 copy.96
  423.6 5.1 %all-to-all-start.2 = ((bf16[128,4,2048]{2,1,0:T(4,128)(2,1)}), bf16[128,4,2048]{2,1,0:T(4,128)(2,1)}, u32[]{:S(2)}, u32[]{:S(2)}) async-start(bf16[128,4,2048]{2,1,0:T(4,128)(2,1)} %copy.96), calls=%async_computation.3 | async-start | bytes 4194304 | tf_op jit(solution)/shard_map/all_to_all | solution.py:211
  428.8 30.3 %all-to-all-done.2 = bf16[128,4,2048]{2,1,0:T(4,128)(2,1)} async-done(((bf16[128,4,2048]{2,1,0:T(4,128)(2,1)}), bf16[128,4,2048]{2,1,0:T(4,128)(2,1)}, u32[]{:S(2)}, u32[]{:S(2)}) %all-to-all-start.2) | async-done | bytes 2097184 | tf_op jit(solution)/shard_map/all_to_all | solution.py:211
  459.1 4.0 reshape.464
  463.1 5.2 %gather_fusion = bf16[256,2048]{1,0:T(8,128)(2,1)} fusion(bf16[512,2048]{1,0:T(8,128)(2,1)} %reshape.464, s32[1024]{0:T(1024)S(1)} %pad_clamp_fusion), kind=kCustom, calls=%fused_computation | custom fusion | bytes 2098176 | tf_op jit(solution)/shard_map/gather | solution.py:218
  468.3 3.4 reshape.468
  471.7 4.8 multiply_reduce_fusion
  (390 shorter events, 189.3 us)
Async XLA Ops:
  6.5 405.0 %copy-start = (bf16[1,512,2048]{2,1,0:T(8,128)(2,1)S(1)}, bf16[1,512,2048]{2,1,0:T(8,128)(2,1)}, u32[]{:S(2)}) copy-start(bf16[1,512,2048]{2,1,0:T(8,128)(2,1)} %param.37) | copy-start | bytes 6291460
  6.5 2.9 copy-start.7
  6.5 3.9 copy-start.6
  6.5 4.0 copy-start.8
  6.5 60.5 %all-gather.3.cloned.1.call-start = ((), (), s32[]{:S(2)}) async-start(), calls=%async_computation.4 | async-start | bytes 8650752 | tf_op jit(solution)/shard_map/all_gather | solution.py:20
  6.6 35.9 %copy-start.15 = (f32[128]{0:T(128)S(1)}, f32[128]{0:T(128)}, u32[]{:S(2)}) copy-start(f32[128]{0:T(128)} %param.26) | copy-start | bytes 1540
  10.3 341.9 %reduce-scatter.2.cloned.1.call-start = ((), (), s32[]{:S(2)}) async-start(), calls=%async_computation.5 | async-start | bytes 2621440 | tf_op jit(solution)/shard_map/reduce_scatter | solution.py:165
  76.0 2.7 copy-start.1
  83.0 2.7 copy-start.1
  90.6 2.7 copy-start.1
  98.3 2.7 copy-start.1
  105.9 2.7 copy-start.1
  113.5 2.7 copy-start.1
  121.1 2.7 copy-start.1
  128.8 2.7 copy-start.1
  136.4 2.7 copy-start.1
  144.0 2.7 copy-start.1
  151.7 2.7 copy-start.1
  159.3 2.7 copy-start.1
  166.9 2.7 copy-start.1
  174.5 2.7 copy-start.1
  182.2 2.7 copy-start.1
  189.8 2.7 copy-start.1
  197.4 2.7 copy-start.1
  205.1 2.7 copy-start.1
  212.7 2.7 copy-start.1
  220.3 2.7 copy-start.1
  228.0 2.7 copy-start.1
  235.6 2.7 copy-start.1
  243.2 2.7 copy-start.1
  250.8 2.7 copy-start.1
  258.5 2.7 copy-start.1
  266.1 2.7 copy-start.1
  273.7 2.7 copy-start.1
  281.4 2.7 copy-start.1
  289.0 2.7 copy-start.1
  296.6 2.7 copy-start.1
  304.2 2.7 copy-start.1
  311.9 2.7 copy-start.1
  323.3 28.9 %copy-start.2 = (bf16[128,2048]{1,0:T(8,128)(2,1)S(1)}, bf16[128,2048]{1,0:T(8,128)(2,1)}, u32[]{:S(2)}) copy-start(bf16[128,2048]{1,0:T(8,128)(2,1)} %param.30) | copy-start | bytes 1572868
  324.0 31.1 %copy-start.9 = (f32[2048]{0:T(1024)S(1)}, f32[2048]{0:T(1024)}, u32[]{:S(2)}) copy-start(f32[2048]{0:T(1024)} %param.32) | copy-start | bytes 24580
  324.0 31.1 %copy-start.10 = (f32[2048]{0:T(1024)S(1)}, f32[2048]{0:T(1024)}, u32[]{:S(2)}) copy-start(f32[2048]{0:T(1024)} %param.31) | copy-start | bytes 24580
  325.3 8.0 %all-to-all-start = ((f32[4,1,128]{2,1,0:T(1,128)}), f32[4,1,128]{2,1,0:T(1,128)S(1)}, u32[]{:S(2)}, u32[]{:S(2)}) async-start(f32[4,1,128]{2,1,0:T(1,128)} %bitcast.17), calls=%async_computation.1 | async-start | bytes 4096 | tf_op jit(solution)/shard_map/all_to_all | solution.py:31
  352.2 2.9 copy-start.3
  368.0 40.1 %copy-start.16 = (bf16[1,2048,512]{2,1,0:T(8,128)(2,1)S(1)}, bf16[1,2048,512]{2,1,0:T(8,128)(2,1)}, u32[]{:S(2)}) copy-start(bf16[1,2048,512]{2,1,0:T(8,128)(2,1)} %param.35) | copy-start | bytes 6291460
  406.9 1.3 copy-start.4
  423.6 5.1 %copy-start.14 = (f32[128,2]{0,1:T(2,128)S(1)}, f32[128,2]{0,1:T(2,128)}, u32[]{:S(2)}) copy-start(f32[128,2]{0,1:T(2,128)} %param.34) | copy-start | bytes 3076
  423.6 35.5 %all-to-all-start.2 = ((bf16[128,4,2048]{2,1,0:T(4,128)(2,1)}), bf16[128,4,2048]{2,1,0:T(4,128)(2,1)}, u32[]{:S(2)}, u32[]{:S(2)}) async-start(bf16[128,4,2048]{2,1,0:T(4,128)(2,1)} %copy.96), calls=%async_computation.3 | async-start | bytes 4194304 | tf_op jit(solution)/shard_map/all_to_all | solution.py:211
  (4 other events, 2.9 us)
Sparse Core Ops, SparseCore 0:
  10.5 56.5 all-gather.2
  323.5 28.6 reduce-scatter.1
where the time goes:
time: 488 us; the launch traced here: 485 us
  matrix products  190 us (39%)
  other arithmetic  80.6 us (17%)
  waiting for transfers between devices  77.6 us (16%)
  blocking collectives  65.9 us (14%)
  local copies, waits for them, and re-layouts  44.3 us (9%)
  between operations  16.1 us (3%)
  starting transfers between devices  9.12 us (2%)
    dot_general x32, matrix products, advance(): jnp.einsum('qkgd,tkd->kgqt', query_rot, key_block, preferred_element_type...  89.6 us
    dot_general x32, matrix products, advance(): jnp.einsum('kgqt,tkd->kgqd', weights.astype(jnp.bfloat16), value_block, p...  86.5 us
    add x32, other arithmetic, advance(): new_total = running_total * rescale + jnp.sum(weights, axis=-1)  40.1 us
    all_to_all x1, blocking collectives, per_device(): lax.all_to_all(outbound.reshape(expert_total, capacity, model_width), ('s...  38.8 us
    all_to_all x1, waiting for transfers between devices, per_device(): lax.all_to_all(served.astype(jnp.bfloat16).reshape(arrived.shape), ('sp',...  30.3 us
    all_gather x1, blocking collectives, per_device(): lax.all_gather(documents, 'sp', axis=0, tiled=True)  27.1 us
    all_gather x1, waiting for transfers between devices, sent_together(): filled = lax.all_gather(both, axis, axis=dim, tiled=True)  24.3 us
    reduce_scatter x1, waiting for transfers between devices, per_device(): lax.psum_scatter(jnp.dot(scaled, own_rows, preferred_element_type=jnp.flo...  18.9 us
  transfers between devices with their start and end apart: 4, of which 4 were waited for; matrix products, arithmetic and copies ran while one was open for 1% of the time, Pallas kernels for 0%

commit v1 on v0

v1 whole, which is shorter than its diff:
```python
import functools
import math

import jax
import jax.numpy as jnp
import numpy as np
from jax import lax
from jax.experimental import pallas as pl
from jax.experimental.pallas import tpu as pltpu
from jax.sharding import PartitionSpec as P

HEAD = 128
GRID = 64
KEY_BLOCK = 1152
ALIGN = 128

eps_norm = 1e-06
alpha_mix = 8.0**0.25
theta_base = 10000.0
LOG2_SCALE = HEAD ** (-0.5) * math.log2(math.e)

ANY = pl.BlockSpec(memory_space=pl.ANY)
VMEM = pl.BlockSpec(memory_space=pltpu.VMEM)


def rotary_tables(row_total, offset):
    positions = offset + jnp.arange(row_total, dtype=jnp.int32)
    grid_row = (positions // GRID).astype(jnp.float32)
    grid_col = (positions % GRID).astype(jnp.float32)
    pair_count = HEAD // 4
    inv_freq = theta_base ** (-jnp.arange(pair_count, dtype=jnp.float32) / pair_count)
    angles = jnp.concatenate(
        [grid_row[:, None] * inv_freq[None, :], grid_col[:, None] * inv_freq[None, :]], axis=1
    )
    cosine, sine = jnp.cos(angles), jnp.sin(angles)
    return jnp.concatenate([cosine, cosine], axis=1), jnp.concatenate([-sine, sine], axis=1)


def turn(values, gain, cosine, sine):
    inv_rms = lax.rsqrt(jnp.mean(values * values, axis=-1, keepdims=True) + eps_norm)
    values = values * inv_rms * gain
    swapped = pltpu.roll(values, HEAD // 2, 1)
    return (values * cosine + swapped * sine).astype(jnp.bfloat16)


def key_kernel(key_ref, value_ref, docs_ref, gain_ref, cos_ref, sin_ref, out_ref):
    rows = key_ref.shape[0]
    out_ref[0:rows, 0:HEAD] = turn(
        key_ref[...].astype(jnp.float32), gain_ref[...], cos_ref[...], sin_ref[...]
    )
    out_ref[0:rows, HEAD:] = value_ref[...]
    out_ref[rows:, :] = jnp.zeros((out_ref.shape[0] - rows, out_ref.shape[1]), jnp.bfloat16)
    docs = docs_ref[...].astype(jnp.float32)
    padded = jnp.concatenate([docs, jnp.zeros((16 - docs.shape[0], docs.shape[1]), jnp.float32)], axis=0)
    out_ref[rows:, :] = padded.astype(jnp.bfloat16)


def query_kernel(query_ref, gain_ref, cos_ref, sin_ref, out_ref):
    for head in range(out_ref.shape[0]):
        out_ref[head] = turn(
            query_ref[:, head * HEAD : (head + 1) * HEAD].astype(jnp.float32),
            gain_ref[...],
            cos_ref[...],
            sin_ref[...],
        )


def attention_kernel(shards, rows, tile, q_ref, docs_ref, kv_ref, out_ref, k_buf, v_buf, d_buf, start_buf, end_buf, acc, top, sem):
    heads = q_ref.shape[0]
    total_keys = shards * rows
    doc_copy = pltpu.make_async_copy(kv_ref.at[:, pl.ds(rows, 16), :], d_buf, sem.at[2 * shards])
    doc_copy.start()
    v_buf[:, HEAD:] = jnp.ones((v_buf.shape[0], HEAD), jnp.bfloat16)
    v_buf[total_keys:, 0:HEAD] = jnp.zeros((KEY_BLOCK, HEAD), jnp.bfloat16)
    doc_copy.wait()
    all_docs = d_buf[:, 0:8, :].astype(jnp.float32).astype(jnp.int32)[:, 0:2, :]
    docs_here = docs_ref[...]
    half = rows // 2

    counts = [
        jnp.sum(jnp.sum((all_docs < d).astype(jnp.float32), axis=(0, 1), keepdims=False)[None, :], axis=1, keepdims=True)
        for d in range(1, 9)
    ]
    counts = [jnp.zeros((1, 1), jnp.float32)] + counts + [jnp.full((1, 1), float(total_keys), jnp.float32)]
    bounds = []
    for t in range(rows // tile):
        per_row = half // tile
        mine = docs_here[t // per_row : t // per_row + 1, (t % per_row) * tile : (t % per_row + 1) * tile]
        start_row = jnp.zeros(mine.shape, jnp.float32)
        end_row = jnp.zeros(mine.shape, jnp.float32)
        for d in range(9):
            start_row = jnp.where(mine == d, counts[d], start_row)
            end_row = jnp.where(mine == d, counts[d + 1], end_row)
        for row, buf in ((start_row, start_buf), (end_row, end_buf)):
            column = jnp.transpose(jnp.broadcast_to(row, (HEAD, tile))).astype(jnp.int32)
            buf[t * tile : (t + 1) * tile, :] = column
        start, last_start = jnp.min(start_row).astype(jnp.int32), jnp.max(start_row).astype(jnp.int32)
        bounds.append((start, jnp.max(end_row).astype(jnp.int32), start == last_start))

    def base_of(t):
        return (bounds[t][0] // ALIGN) * ALIGN

    def blocks_of(t):
        return (bounds[t][1] - base_of(t) + KEY_BLOCK - 1) // KEY_BLOCK

    first_shard = base_of(0) // rows
    limit = base_of(0)
    for t in range(rows // tile):
        limit = jnp.maximum(limit, base_of(t) + blocks_of(t) * KEY_BLOCK)
    last_shard = jnp.minimum((limit + rows - 1) // rows, shards)

    def k_copy(s):
        return pltpu.make_async_copy(
            kv_ref.at[s, pl.ds(0, rows), pl.ds(0, HEAD)],
            k_buf.at[pl.ds(pl.multiple_of(s * rows, rows), rows), :],
            sem.at[s],
        )

    def v_copy(s):
        return pltpu.make_async_copy(
            kv_ref.at[s, pl.ds(0, rows), pl.ds(HEAD, HEAD)],
            v_buf.at[pl.ds(pl.multiple_of(s * rows, rows), rows), pl.ds(0, HEAD)],
            sem.at[shards + s],
        )

    @pl.loop(first_shard, last_shard)
    def _(s):
        k_copy(s).start()
        v_copy(s).start()

    waited = first_shard
    for t in range(rows // tile):
        base = base_of(t)
        q = q_ref[:, t * tile : (t + 1) * tile, :].reshape(heads * tile, HEAD)
        acc[...] = jnp.zeros_like(acc)
        top[...] = jnp.full_like(top, -1e30)
        start, end, single = bounds[t]

        def advance(q, offset, masked, t=t):
            offset = pl.multiple_of(offset, ALIGN)
            keys = k_buf[pl.ds(offset, KEY_BLOCK), :]
            values = v_buf[pl.ds(offset, KEY_BLOCK), :]
            scores = lax.dot_general(q, keys, (((1,), (1,)), ((), ())), preferred_element_type=jnp.float32)
            if masked:
                place = offset + lax.broadcasted_iota(jnp.int32, (heads * tile, KEY_BLOCK), 1)
                reps = KEY_BLOCK // HEAD

                def spread(buf):
                    one = buf[t * tile : (t + 1) * tile, :]
                    both = jnp.concatenate([one] * heads, axis=0)
                    return jnp.concatenate([both] * reps, axis=1)

                allowed = (place >= spread(start_buf)) & (place < spread(end_buf))
                scores = jnp.where(allowed, scores, -1e30)
            old = top[...]
            new = jnp.maximum(old, jnp.max(scores, axis=1, keepdims=True))
            shift = jnp.concatenate([new * LOG2_SCALE] * (KEY_BLOCK // HEAD), axis=1)
            weights = jnp.exp2(scores * LOG2_SCALE - shift)
            if masked:
                weights = jnp.where(allowed, weights, 0.0)
            rescale = jnp.exp2((old - new) * LOG2_SCALE)
            part = jnp.dot(weights.astype(jnp.bfloat16), values, preferred_element_type=jnp.float32)
            acc[...] = acc[...] * jnp.concatenate([rescale, rescale], axis=1) + part
            top[...] = new

        def step(b, waited):
            offset = base + b * KEY_BLOCK
            need = jnp.minimum((offset + KEY_BLOCK + rows - 1) // rows, shards)

            @pl.loop(waited, need)
            def _(s):
                k_copy(s).wait()
                v_copy(s).wait()

            inside = single & (offset >= start) & (offset + KEY_BLOCK <= end)

            @pl.when(inside)
            def _():
                advance(q, offset, False)

            @pl.when(jnp.logical_not(inside))
            def _():
                advance(q, offset, True)

            return jnp.maximum(waited, need)

        waited = lax.fori_loop(0, blocks_of(t), step, waited)
        result = (acc[:, 0:HEAD] / acc[:, HEAD:]).astype(jnp.bfloat16)
        for head in range(heads):
            out_ref[t * tile : (t + 1) * tile, head * HEAD : (head + 1) * HEAD] = result[head * tile : (head + 1) * tile]

    @pl.loop(waited, last_shard)
    def _(s):
        k_copy(s).wait()
        v_copy(s).wait()


def layer_norm(stream, gain_vec, bias_vec):
    center = jnp.mean(stream, axis=-1, keepdims=True)
    spread = jnp.mean(jnp.square(stream - center), axis=-1, keepdims=True)
    return (stream - center) * lax.rsqrt(spread + eps_norm) * gain_vec + bias_vec


def attend(queries, key_heads, value_heads, documents, query_gain, key_gain):
    rows = queries.shape[0]
    heads = queries.shape[1] // HEAD
    shards = lax.axis_size("sp")
    cosine, sine = rotary_tables(rows, lax.axis_index("sp") * rows)
    docs = documents.reshape(2, rows // 2)
    sent = pl.pallas_call(
        key_kernel,
        out_shape=jax.ShapeDtypeStruct((rows + 16, 2 * HEAD), jnp.bfloat16),
        in_specs=[VMEM] * 6,
        out_specs=VMEM,
        cost_estimate=pl.CostEstimate(flops=1000000, bytes_accessed=1000000, transcendentals=0),
        name="keys",
    )(key_heads, value_heads, docs, key_gain.reshape(1, HEAD), cosine, sine)
    filled = lax.all_gather(sent, "sp", axis=0, tiled=False)
    query_rot = pl.pallas_call(
        query_kernel,
        out_shape=jax.ShapeDtypeStruct((heads, rows, HEAD), jnp.bfloat16),
        in_specs=[VMEM] * 4,
        out_specs=VMEM,
        cost_estimate=pl.CostEstimate(flops=1000000, bytes_accessed=1000000, transcendentals=0),
        name="queries",
    )(queries, query_gain.reshape(1, HEAD), cosine, sine)
    tile = rows // 2
    return pl.pallas_call(
        functools.partial(attention_kernel, shards, rows, tile),
        out_shape=jax.ShapeDtypeStruct((rows, heads * HEAD), jnp.bfloat16),
        in_specs=[VMEM, VMEM, ANY],
        out_specs=VMEM,
        scratch_shapes=[
            pltpu.VMEM((shards * rows + KEY_BLOCK, HEAD), jnp.bfloat16),
            pltpu.VMEM((shards * rows + KEY_BLOCK, 2 * HEAD), jnp.bfloat16),
            pltpu.VMEM((shards, 16, 2 * HEAD), jnp.bfloat16),
            pltpu.VMEM((rows, HEAD), jnp.int32),
            pltpu.VMEM((rows, HEAD), jnp.int32),
            pltpu.VMEM((heads * tile, 2 * HEAD), jnp.float32),
            pltpu.VMEM((heads * tile, HEAD), jnp.float32),
            pltpu.SemaphoreType.DMA((2 * shards + 1,)),
        ],
        compiler_params=pltpu.CompilerParams(vmem_limit_bytes=56 * 1024 * 1024),
        cost_estimate=pl.CostEstimate(flops=6000000000, bytes_accessed=9000000, transcendentals=11000000),
        name="attention",
    )(query_rot, docs, filled)


def per_device(
    queries,
    key_heads,
    value_heads,
    documents,
    query_gain,
    key_gain,
    out_gain,
    out_proj,
    residual,
    mid_gain,
    mid_bias,
    routes,
    route_weights,
    expert_gate,
    expert_up,
    expert_down,
    final_gain,
    final_bias,
):
    attention = attend(queries, key_heads, value_heads, documents, query_gain, key_gain)
    tp_size = lax.axis_size("tp")
    tiles = attention.reshape(tp_size, attention.shape[0] // tp_size, attention.shape[1])
    arrived = lax.all_to_all(tiles, "tp", split_axis=0, concat_axis=0, tiled=True)
    attention = jnp.transpose(arrived, (1, 0, 2)).reshape(arrived.shape[1], -1)
    attn_float = attention.astype(jnp.float32)
    mean_square = jnp.mean(attn_float * attn_float, axis=1, keepdims=True)
    scaled = (attn_float * out_gain).astype(jnp.bfloat16)
    projected = jnp.dot(scaled, out_proj, preferred_element_type=jnp.float32)
    projected = projected * lax.rsqrt(mean_square + eps_norm)
    middle = layer_norm(
        alpha_mix * residual.astype(jnp.float32) + projected, mid_gain, mid_bias
    ).astype(jnp.bfloat16)
    out_rows = middle.shape[0]
    model_width = middle.shape[1]
    top_count = routes.shape[1]
    local_experts = expert_gate.shape[0]
    sp_size = lax.axis_size("sp")
    tp_size = lax.axis_size("tp")
    expert_total = local_experts * sp_size * tp_size
    capacity = 2 * out_rows * top_count // expert_total
    flat_routes = routes.reshape(-1)
    one_hot = (flat_routes[:, None] == jnp.arange(expert_total, dtype=jnp.int32)[None, :]).astype(
        jnp.int32
    )
    rank_in = jnp.sum((jnp.cumsum(one_hot, axis=0) - one_hot) * one_hot, axis=1)
    target = flat_routes * capacity + rank_in
    outbound = (
        jnp.zeros((expert_total * capacity, model_width), jnp.bfloat16)
        .at[target]
        .set(jnp.repeat(middle, top_count, axis=0))
    )
    arrived = lax.all_to_all(
        outbound.reshape(expert_total, capacity, model_width),
        ("sp", "tp"),
        split_axis=0,
        concat_axis=0,
        tiled=True,
    )
    item_count = arrived.shape[-2]
    grouped_rows = arrived.reshape(-1, local_experts, item_count, model_width)
    gate_part = jnp.einsum(
        "sekd,edf->sekf", grouped_rows, expert_gate, preferred_element_type=jnp.float32
    )
    up_part = jnp.einsum(
        "sekd,edf->sekf", grouped_rows, expert_up, preferred_element_type=jnp.float32
    )
    hidden = (jax.nn.silu(gate_part) * up_part).astype(jnp.bfloat16)
    served = jnp.einsum("sekf,efd->sekd", hidden, expert_down, preferred_element_type=jnp.float32)
    returned = lax.all_to_all(
        served.astype(jnp.bfloat16).reshape(arrived.shape),
        ("sp", "tp"),
        split_axis=0,
        concat_axis=0,
        tiled=True,
    )
    picked = returned.reshape(expert_total * capacity, model_width)[target]
    picked = picked.astype(jnp.float32).reshape(out_rows, top_count, model_width)
    routed = jnp.sum(picked * route_weights[:, :, None], axis=1)
    return layer_norm(
        alpha_mix * middle.astype(jnp.float32) + routed, final_gain, final_bias
    ).astype(jnp.bfloat16)


def solution(mesh):
    both = ("sp", "tp")
    return jax.shard_map(
        per_device,
        mesh=mesh,
        in_specs=(
            P("sp", "tp"),
            P("sp", "tp"),
            P("sp", "tp"),
            P("sp"),
            P(),
            P(),
            P(),
            P(),
            P(both, None),
            P(),
            P(),
            P(both, None),
            P(both, None),
            P(both, None, None),
            P(both, None, None),
            P(both, None, None),
            P(),
            P(),
        ),
        out_specs=P(both, None),
        check_vma=False,
    )
```

time: 488 us -> 252 us (0.52)
  matrix products: 190 us -> 14.1 us
  other arithmetic: 80.6 us -> 11.5 us
  Pallas kernels: 0 us -> 17.2 us
  waiting for transfers between devices: 77.6 us -> 89.6 us
  local copies, waits for them, and re-layouts: 44.3 us -> 34.1 us
    dot_general x65 -> x1, matrix products: 179 us -> 3.14 us  [per_device(): projected = jnp.dot(scaled, out_proj, preferred_element_type=jnp.float32)]
    add x32 -> x0, other arithmetic: 40.1 us -> none  [advance(): new_total = running_total * rescale + jnp.sum(weights, axis=-1)]
    all_gather x1, waiting for transfers between devices: 24.3 us -> 53.7 us  [attend(): filled = lax.all_gather(sent, 'sp', axis=0, tiled=False)]
    all_gather x1 -> x0, blocking collectives: 27.1 us -> none  [per_device(): lax.all_gather(documents, 'sp', axis=0, tiled=True)]
    all_to_all x1, blocking collectives: 38.8 us -> 63.8 us  [per_device(): lax.all_to_all(outbound.reshape(expert_total, capacity, model_width), ('s...]
    reduce_sum x36 -> x1, other arithmetic: 19.9 us -> 0.15 us  [per_device(): mean_square = jnp.mean(attn_float * attn_float, axis=1, keepdims=True)]
    reduce_scatter x1 -> x0, waiting for transfers between devices: 18.9 us -> none  [per_device(): lax.psum_scatter(jnp.dot(scaled, own_rows, preferred_element_type=jnp.flo...]
    pallas_call x0 -> x3, Pallas kernels: none -> 17.2 us  [the longest x1 12.8 us: attend(): pl.pallas_call(functools.partial(attention_kernel, shards, rows, tile), o...]
  transfers between devices with their start and end apart: 4 -> 3, of which waited for: 4 -> 3; matrix products, arithmetic and copies ran while one was open for 1% -> 1% of each run, Pallas kernels for 0% -> 1%
where the time goes in v1:
time: 252 us; the launch traced here: 253 us
  waiting for transfers between devices  89.6 us (36%)
  blocking collectives  63.8 us (25%)
  local copies, waits for them, and re-layouts  34.1 us (14%)
  Pallas kernels  17.2 us (7%)
  matrix products  14.1 us (6%)
  between operations  13.6 us (5%)
  other arithmetic  11.5 us (5%)
  starting transfers between devices  9.07 us (4%)
    all_to_all x1, blocking collectives, per_device(): lax.all_to_all(outbound.reshape(expert_total, capacity, model_width), ('s...  63.8 us
    all_gather x1, waiting for transfers between devices, attend(): filled = lax.all_gather(sent, 'sp', axis=0, tiled=False)  53.7 us
    all_to_all x1, waiting for transfers between devices, per_device(): lax.all_to_all(served.astype(jnp.bfloat16).reshape(arrived.shape), ('sp',...  30.3 us
    pallas_call x1, Pallas kernels, attend(): pl.pallas_call(functools.partial(attention_kernel, shards, rows, tile), o...  12.8 us
    dot_general x1, matrix products, per_device(): jnp.einsum('sekf,efd->sekd', hidden, expert_down, preferred_element_type=...  7.52 us
    all_to_all x1, waiting for transfers between devices, per_device(): lax.all_to_all(tiles, 'tp', split_axis=0, concat_axis=0, tiled=True)  5.52 us
    gather x1, local copies, waits for them, and re-layouts, per_device(): picked = returned.reshape(expert_total * capacity, model_width)[target]  5.2 us
    all_to_all x1, starting transfers between devices, per_device(): lax.all_to_all(served.astype(jnp.bfloat16).reshape(arrived.shape), ('sp',...  5.1 us
  transfers between devices with their start and end apart: 3, of which 3 were waited for; matrix products, arithmetic and copies ran while one was open for 1% of the time, Pallas kernels for 1%

profile of v1, /device:TPU:1, one launch (start us, length us, event | category | flops | bytes accessed | tf_op | source)
XLA Modules:
  0.0 252.9 jit_solution(16066793479535223502)
XLA Ops:
  6.6 0.2 broadcast_multiply_fusion.1
  6.8 1.1 fusion.55
  7.9 0.8 pad_maximum_fusion.1.cos_ref
  8.8 0.6 reshape.175.docs_ref
  9.4 0.9 pad_maximum_fusion.2.sin_ref
  10.2 2.1 keys.1
  12.4 0.0 all-gather.3.cloned.1.call-update
  12.4 0.1 copy.31
  12.5 0.1 eq.31
  12.7 0.1 eq.27
  12.8 0.1 copy.30
  12.9 0.1 mul.141
  13.1 0.1 copy.33
  13.2 0.2 fusion.42
  13.5 2.2 queries.1.q_ref
  15.7 0.2 fusion.44
  15.9 53.7 %all-gather.3.cloned.1.call-done = bf16[16896,256]{1,0:T(8,128)(2,1)} async-done(((bf16[528,256]{1,0:T(8,128)(2,1)}), bf16[16896,256]{1,0:T(8,128)(2,1)}) %all-gather.3.cloned.1.call-update) | async-done | bytes 8650768 | tf_op jit(solution)/shard_map/all_gather | solution.py:218
  69.6 12.8 %attention.1 = bf16[512,256]{1,0:T(8,128)(2,1)} custom-call(bf16[2,512,128]{2,1,0:T(8,128)(2,1)} %queries.1.q_ref, s32[2,256]{1,0:T(2,128)} %reshape.175.docs_ref, bf16[32,528,256]{2,1,0:T(8,128)(2,1)} %bitcast.84), custom_call_target="tpu_custom_call" | custom-call | flops 6000000000 | bytes 9000000 | tf_op jit(solution)/shard_map/attention/pallas_call | solution.py:228
  82.5 1.8 copy.29
  84.3 4.0 %all-to-all-start = ((bf16[4,128,256]{1,2,0:T(8,128)(2,1)}), bf16[4,128,256]{1,2,0:T(8,128)(2,1)S(1)}, u32[]{:S(2)}, u32[]{:S(2)}) async-start(bf16[4,128,256]{1,2,0:T(8,128)(2,1)} %copy.29), calls=%async_computation | async-start | bytes 524288 | tf_op jit(solution)/shard_map/all_to_all | solution.py:272
  88.2 5.5 %all-to-all-done = bf16[4,128,256]{1,2,0:T(8,128)(2,1)S(1)} async-done(((bf16[4,128,256]{1,2,0:T(8,128)(2,1)}), bf16[4,128,256]{1,2,0:T(8,128)(2,1)S(1)}, u32[]{:S(2)}, u32[]{:S(2)}) %all-to-all-start) | async-done | bytes 262176 | tf_op jit(solution)/shard_map/all_to_all | solution.py:272
  93.8 0.2 multiply_reduce_fusion.3
  93.9 0.2 fusion.39
  94.1 0.0 copy-start.2
  94.2 3.1 %fusion.57 = (f32[128]{0:T(128)S(1)}, f32[128,2048]{1,0:T(8,128)S(1)}) fusion(f32[128]{0:T(128)S(1)} %add_rsqrt_fusion.2, bf16[128,1024]{0,1:T(8,128)(2,1)S(1)} %fusion.39, bf16[1024,2048]{1,0:T(8,128)(2,1)} %param.25, bf16[128,2048]{1,0:T(8,128)(2,1)} %param.26), kind=kOutput, calls=%fused_computation.70 | convolution fusion | flops 538181504 | bytes 6030336 | tf_op jit(solution)/shard_map/dot_general | solution.py:277
  97.3 0.3 multiply_reduce_fusion.2
  97.6 0.2 add_convert_fusion.1
  97.8 1.6 broadcast_in_dim.5
  99.5 2.3 reshape.200
  101.7 4.4 %scatter_custom_fusion = bf16[512,2048]{1,0:T(8,128)(2,1)} fusion(s32[256]{0:T(256)S(1)} %bitcast.80, bf16[256,2048]{1,0:T(8,128)(2,1)} %reshape.200, bf16[]{:T(256)} %constant.67.clone.1), kind=kCustom, calls=%fused_computation.20 | custom fusion | bytes 2097664 | tf_op jit(solution)/shard_map/scatter | solution.py:299
  106.2 4.1 %reshape.180 = bf16[128,4,2048]{2,1,0:T(4,128)(2,1)} reshape(bf16[512,2048]{1,0:T(8,128)(2,1)} %scatter_custom_fusion) | data formatting | bytes 4194304 | tf_op jit(solution)/shard_map/reshape | solution.py:302
  110.3 63.8 %all_to_all.15 = bf16[128,4,2048]{2,1,0:T(4,128)(2,1)S(1)} all-to-all(bf16[128,4,2048]{2,1,0:T(4,128)(2,1)} %reshape.180), channel_id=1, replica_groups=mesh['sp'=32,'tp'=4] {'sp','tp'}, dimensions={0} | all-to-all | bytes 4194304 | tf_op jit(solution)/shard_map/all_to_all | solution.py:301
  174.1 1.3 copy-done.1
  175.4 3.4 %fusion.8 = f32[128,1,4,512]{3,0,2,1:T(8,128)} fusion(bf16[1,2048,512]{2,1,0:T(8,128)(2,1)S(1)} %copy-done.10, bf16[128,4,2048]{2,1,0:T(4,128)(2,1)S(1)} %all_to_all.15), kind=kOutput, calls=%fused_computation.13 | convolution fusion | flops 1073741824 | bytes 5242880 | tf_op jit(solution)/shard_map/sekd,edf->sekf/dot_general | solution.py:310
  178.8 7.5 %convolution_convert_fusion = bf16[128,4,2048]{2,0,1:T(8,128)(2,1)} fusion(bf16[1,512,2048]{2,1,0:T(8,128)(2,1)S(1)} %copy-done, bf16[1,2048,512]{2,1,0:T(8,128)(2,1)} %param.32, bf16[128,4,2048]{2,1,0:T(4,128)(2,1)} %copy-done.1, f32[128,1,4,512]{3,0,2,1:T(8,128)} %fusion.8), kind=kOutput, calls=%fused_computation.2 | convolution fusion | flops 2150105088 | bytes 9437184 | tf_op jit(solution)/shard_map/sekf,efd->sekd/dot_general | solution.py:317
  186.3 4.5 %copy.37 = bf16[128,4,2048]{2,1,0:T(4,128)(2,1)} copy(bf16[128,4,2048]{2,0,1:T(8,128)(2,1)} %convolution_convert_fusion) | data formatting | bytes 4194304 | tf_op jit(solution)/shard_map/convert_element_type | solution.py:319
  190.8 5.1 %all-to-all-start.2 = ((bf16[128,4,2048]{2,1,0:T(4,128)(2,1)}), bf16[128,4,2048]{2,1,0:T(4,128)(2,1)}, u32[]{:S(2)}, u32[]{:S(2)}) async-start(bf16[128,4,2048]{2,1,0:T(4,128)(2,1)} %copy.37), calls=%async_computation.2 | async-start | bytes 4194304 | tf_op jit(solution)/shard_map/all_to_all | solution.py:318
  195.9 0.1 copy.38
  196.1 30.3 %all-to-all-done.2 = bf16[128,4,2048]{2,1,0:T(4,128)(2,1)} async-done(((bf16[128,4,2048]{2,1,0:T(4,128)(2,1)}), bf16[128,4,2048]{2,1,0:T(4,128)(2,1)}, u32[]{:S(2)}, u32[]{:S(2)}) %all-to-all-start.2) | async-done | bytes 2097184 | tf_op jit(solution)/shard_map/all_to_all | solution.py:318
  226.3 4.0 %reshape.185 = bf16[512,2048]{1,0:T(8,128)(2,1)} reshape(bf16[128,4,2048]{2,1,0:T(4,128)(2,1)} %all-to-all-done.2) | data formatting | bytes 4194304 | tf_op jit(solution)/shard_map/reshape | solution.py:325
  230.3 5.2 %gather_fusion = bf16[256,2048]{1,0:T(8,128)(2,1)} fusion(bf16[512,2048]{1,0:T(8,128)(2,1)} %reshape.185, s32[1024]{0:T(1024)S(1)} %pad_clamp_fusion), kind=kCustom, calls=%fused_computation | custom fusion | bytes 2098176 | tf_op jit(solution)/shard_map/gather | solution.py:325
  235.5 3.4 %reshape.187 = f32[128,2,2048]{2,1,0:T(2,128)} reshape(bf16[256,2048]{1,0:T(8,128)(2,1)} %gather_fusion) | data formatting | bytes 3145728 | tf_op jit(solution)/shard_map/convert_element_type | solution.py:326
  238.9 4.8 %multiply_reduce_fusion = f32[128,2048]{1,0:T(8,128)S(1)} fusion(f32[128,2,2048]{2,1,0:T(2,128)} %reshape.187, f32[128,2]{1,0:T(8,128)S(1)} %copy.38), kind=kLoop, calls=%fused_computation.10 | loop fusion | flops 786432 | bytes 3146752 | tf_op jit(solution)/shard_map/reduce_sum | solution.py:327
  243.7 0.0 copy-start.4
  243.7 0.0 copy-start.5
  243.8 0.4 fusion.41
  244.2 0.5 multiply_reduce_fusion.1
  244.7 1.4 add_convert_fusion
  (35 shorter events, 0.2 us)
Async XLA Ops:
  6.5 172.3 %copy-start = (bf16[1,512,2048]{2,1,0:T(8,128)(2,1)S(1)}, bf16[1,512,2048]{2,1,0:T(8,128)(2,1)}, u32[]{:S(2)}) copy-start(bf16[1,512,2048]{2,1,0:T(8,128)(2,1)} %param.33) | copy-start | bytes 6291460
  6.5 2.2 copy-start.8
  6.5 63.1 %all-gather.3.cloned.1.call-start = ((), (), s32[]{:S(2)}) async-start(), calls=%async_computation.3 | async-start | bytes 8921088 | tf_op jit(solution)/shard_map/all_gather | solution.py:218
  6.8 5.6 %copy-start.7 = (s32[128,2]{0,1:T(2,128)S(1)}, s32[128,2]{0,1:T(2,128)}, u32[]{:S(2)}) copy-start(s32[128,2]{0,1:T(2,128)} %param.29) | copy-start | bytes 3076
  69.6 24.3 %copy-start.6 = (f32[1024]{0:T(1024)S(1)}, f32[1024]{0:T(1024)}, u32[]{:S(2)}) copy-start(f32[1024]{0:T(1024)} %param.24) | copy-start | bytes 12292
  84.3 9.5 %all-to-all-start = ((bf16[4,128,256]{1,2,0:T(8,128)(2,1)}), bf16[4,128,256]{1,2,0:T(8,128)(2,1)S(1)}, u32[]{:S(2)}, u32[]{:S(2)}) async-start(bf16[4,128,256]{1,2,0:T(8,128)(2,1)} %copy.29), calls=%async_computation | async-start | bytes 524288 | tf_op jit(solution)/shard_map/all_to_all | solution.py:272
  94.1 3.4 %copy-start.2 = (f32[2048]{0:T(1024)S(1)}, f32[2048]{0:T(1024)}, u32[]{:S(2)}) copy-start(f32[2048]{0:T(1024)} %param.28) | copy-start | bytes 24580
  94.1 3.4 %copy-start.3 = (f32[2048]{0:T(1024)S(1)}, f32[2048]{0:T(1024)}, u32[]{:S(2)}) copy-start(f32[2048]{0:T(1024)} %param.27) | copy-start | bytes 24580
  110.3 65.1 %copy-start.10 = (bf16[1,2048,512]{2,1,0:T(8,128)(2,1)S(1)}, bf16[1,2048,512]{2,1,0:T(8,128)(2,1)}, u32[]{:S(2)}) copy-start(bf16[1,2048,512]{2,1,0:T(8,128)(2,1)} %param.31) | copy-start | bytes 6291460
  174.1 1.3 copy-start.1
  190.8 5.1 %copy-start.9 = (f32[128,2]{0,1:T(2,128)S(1)}, f32[128,2]{0,1:T(2,128)}, u32[]{:S(2)}) copy-start(f32[128,2]{0,1:T(2,128)} %param.30) | copy-start | bytes 3076
  190.8 35.5 %all-to-all-start.2 = ((bf16[128,4,2048]{2,1,0:T(4,128)(2,1)}), bf16[128,4,2048]{2,1,0:T(4,128)(2,1)}, u32[]{:S(2)}, u32[]{:S(2)}) async-start(bf16[128,4,2048]{2,1,0:T(4,128)(2,1)} %copy.37), calls=%async_computation.2 | async-start | bytes 4194304 | tf_op jit(solution)/shard_map/all_to_all | solution.py:318
  243.7 0.9 copy-start.4
  243.7 0.9 copy-start.5
Sparse Core Ops, SparseCore 0:
  12.5 57.0 all-gather.2

commit v2 on v1

--- a/solution.py
+++ b/solution.py
@@ -23,46 +23,11 @@
 VMEM = pl.BlockSpec(memory_space=pltpu.VMEM)
 
 
-def rotary_tables(row_total, offset):
-    positions = offset + jnp.arange(row_total, dtype=jnp.int32)
-    grid_row = (positions // GRID).astype(jnp.float32)
-    grid_col = (positions % GRID).astype(jnp.float32)
-    pair_count = HEAD // 4
-    inv_freq = theta_base ** (-jnp.arange(pair_count, dtype=jnp.float32) / pair_count)
-    angles = jnp.concatenate(
-        [grid_row[:, None] * inv_freq[None, :], grid_col[:, None] * inv_freq[None, :]], axis=1
-    )
-    cosine, sine = jnp.cos(angles), jnp.sin(angles)
-    return jnp.concatenate([cosine, cosine], axis=1), jnp.concatenate([-sine, sine], axis=1)
-
-
 def turn(values, gain, cosine, sine):
     inv_rms = lax.rsqrt(jnp.mean(values * values, axis=-1, keepdims=True) + eps_norm)
     values = values * inv_rms * gain
     swapped = pltpu.roll(values, HEAD // 2, 1)
     return (values * cosine + swapped * sine).astype(jnp.bfloat16)
-
-
-def key_kernel(key_ref, value_ref, docs_ref, gain_ref, cos_ref, sin_ref, out_ref):
-    rows = key_ref.shape[0]
-    out_ref[0:rows, 0:HEAD] = turn(
-        key_ref[...].astype(jnp.float32), gain_ref[...], cos_ref[...], sin_ref[...]
-    )
-    out_ref[0:rows, HEAD:] = value_ref[...]
-    out_ref[rows:, :] = jnp.zeros((out_ref.shape[0] - rows, out_ref.shape[1]), jnp.bfloat16)
-    docs = docs_ref[...].astype(jnp.float32)
-    padded = jnp.concatenate([docs, jnp.zeros((16 - docs.shape[0], docs.shape[1]), jnp.float32)], axis=0)
-    out_ref[rows:, :] = padded.astype(jnp.bfloat16)
-
-
-def query_kernel(query_ref, gain_ref, cos_ref, sin_ref, out_ref):
-    for head in range(out_ref.shape[0]):
-        out_ref[head] = turn(
-            query_ref[:, head * HEAD : (head + 1) * HEAD].astype(jnp.float32),
-            gain_ref[...],
-            cos_ref[...],
-            sin_ref[...],
-        )
 
 
 def attention_kernel(shards, rows, tile, q_ref, docs_ref, kv_ref, out_ref, k_buf, v_buf, d_buf, start_buf, end_buf, acc, top, sem):
@@ -195,37 +160,425 @@
         v_copy(s).wait()
 
 
-def layer_norm(stream, gain_vec, bias_vec):
+NZ, NY, NC, NX = 4, 4, 2, 4
+CAP = 4
+WIDE = 512
+MESH = pl.DeviceIdType.MESH
+
+
+def table_constants():
+    pairs = HEAD // 4
+    inv_freq = (theta_base ** (-np.arange(pairs, dtype=np.float32) / np.float32(pairs))).astype(np.float32)
+    tables = []
+    for count, lane in ((NZ * NY * NC * 8, 0), (GRID, pairs)):
+        angle = np.arange(count, dtype=np.float32)[:, None] * inv_freq[None, :]
+        cosine = np.zeros((count, HEAD), np.float32)
+        sine = np.zeros((count, HEAD), np.float32)
+        for start, sign in ((lane, -1.0), (lane + HEAD // 2, 1.0)):
+            cosine[:, start : start + pairs] = np.cos(angle.astype(np.float64))
+            sine[:, start : start + pairs] = sign * np.sin(angle.astype(np.float64))
+        tables += [cosine, sine]
+    return tables
+
+
+PIECES = ((0, 128), (128, 128), (256, 128), (384, 144))
+
+
+def span(half, part):
+    if part is None:
+        return PIECES[2 * half][0], PIECES[2 * half][1] + PIECES[2 * half + 1][1]
+    return PIECES[2 * half + part]
+
+
+def gather_events():
+    first, second, third, fourth = [], [], [], []
+    for half in (0, 1):
+        first += [(half, 0, 1, None), (half, 0, -1, None), (half, 1, 0, None), (half, -1, 0, None)]
+        second += [(half, 0, 2, 0), (half, 0, 2, 1), (half, 2, 0, 0), (half, 2, 0, 1)]
+        third += [(half, i, j, None) for j in (1, -1) for i in (1, -1)]
+        fourth += [(half, i, 2, p) for p in (0, 1) for i in (1, -1)]
+        fourth += [(half, 2, j, p) for j in (1, -1) for p in (0, 1)]
+    last = [(half, 2, 2, p) for p in (0, 1) for half in (0, 1)]
+    return first + second + third + fourth + last
+
+
+EVENTS = gather_events()
+EVENT_ID = {e: n for n, e in enumerate(EVENTS)}
+
+
+def sends_of(event):
+    half, i, j, part = event
+    out = []
+    if i == 0 and j == 0:
+        out += [(0, s, (half, 0, s, None)) for s in (1, -1)]
+        out += [(1, s, (half, s, 0, None)) for s in (1, -1)]
+    elif i == 0:
+        if j == 1:
+            out.append((0, 1, (half, 0, 2, 0)))
+        if j == -1:
+            out.append((0, -1, (half, 0, 2, 1)))
+        out += [(1, s, (half, s, j, part)) for s in (1, -1)]
+    elif i == 1 and part in (None, 0):
+        out.append((1, 1, (half, 2, j, 0)))
+    elif i == -1 and part in (None, 1):
+        out.append((1, -1, (half, 2, j, 1)))
+    return out
+
+
+SEND_TOTAL = sum(len(sends_of(e)) for e in EVENTS + [(0, 0, 0, None), (1, 0, 0, None)])
+
+
+def gather_kernel(
+    query_ref, key_ref, value_ref, docs_ref, qgain_ref, kgain_ref, rowc_ref, rows_ref, colc_ref, cols_ref,
+    kv_ref, q_ref, own, send_sem, recv_sem, pair_send, pair_recv, local_sem,
+):
+    sp, tp = lax.axis_index("sp"), lax.axis_index("tp")
+    core = sp % NC
+    y = (sp // NC) % NY
+    z = sp // (NC * NY)
+    rows = key_ref.shape[0]
+
+    def shard_at(dz, dy):
+        return ((z + dz + 2 * NZ) % NZ) * (NY * NC) + ((y + dy + 2 * NY) % NY) * NC + core
+
+    partner = sp + 1 - 2 * core
+    barrier = pltpu.get_barrier_semaphore()
+    for dz, dy in ((0, 1), (0, -1), (1, 0), (-1, 0)):
+        pl.semaphore_signal(barrier, inc=1, device_id=(shard_at(dz, dy), tp), device_id_type=MESH)
+    pl.semaphore_signal(barrier, inc=1, device_id=(partner, tp), device_id_type=MESH)
+
+    def table(row_ref, col_ref):
+        near = row_ref[pl.ds(pl.multiple_of(sp * 8, 8), 8), :]
+        return jnp.concatenate([col_ref[...] + near[n : n + 1, :] for n in range(8)], axis=0)
+
+    cosine, sine = table(rowc_ref, colc_ref), table(rows_ref, cols_ref)
+    own[0:rows, 0:HEAD] = turn(key_ref[...].astype(jnp.float32), kgain_ref[...], cosine, sine)
+    own[0:rows, HEAD:] = value_ref[...]
+    docs = docs_ref[...].astype(jnp.float32)
+    padded = jnp.concatenate([docs, jnp.zeros((16 - docs.shape[0], docs.shape[1]), jnp.float32)], axis=0)
+    own[rows:, :] = padded.astype(jnp.bfloat16)
+    pl.semaphore_wait(barrier, 5)
+
+    started = []
+    counter = [0]
+
+    def place(event):
+        half, i, j, part = event
+        return (-i, -j) if half == 0 else (-j, -i)
+
+    def pass_on(event, source):
+        for axis, step, target in sends_of(event):
+            half, i, j, part = target
+            along_y = (axis == 0) == (half == 0)
+            start, size = span(half, part)
+            shard = shard_at(*place(event))
+            dst = kv_ref.at[shard, pl.ds(start, size), :]
+            src = own.at[pl.ds(start, size), :] if source is None else dst
+            copy = pltpu.make_async_remote_copy(
+                src_ref=src,
+                dst_ref=dst,
+                send_sem=send_sem.at[counter[0]],
+                recv_sem=recv_sem.at[EVENT_ID[target]],
+                device_id=(shard_at(0, step) if along_y else shard_at(step, 0), tp),
+                device_id_type=MESH,
+            )
+            counter[0] += 1
+            copy.start()
+            started.append(copy)
+
+    def to_partner(shard, start, size, src, number):
+        copy = pltpu.make_async_remote_copy(
+            src_ref=src,
+            dst_ref=kv_ref.at[shard, pl.ds(start, size), :],
+            send_sem=pair_send.at[number],
+            recv_sem=pair_recv.at[0],
+            device_id=(partner, tp),
+            device_id_type=MESH,
+        )
+        copy.start()
+        started.append(copy)
+
+    for half in (0, 1):
+        pass_on((half, 0, 0, None), None)
+    to_partner(sp, 0, rows + 16, own, len(EVENTS))
+    keep = pltpu.make_async_copy(own, kv_ref.at[sp], local_sem.at[0])
+    keep.start()
+    for head in range(q_ref.shape[0]):
+        q_ref[head] = turn(
+            query_ref[:, head * HEAD : (head + 1) * HEAD].astype(jnp.float32), qgain_ref[...], cosine, sine
+        )
+    for number, event in enumerate(EVENTS):
+        half, i, j, part = event
+        shard = shard_at(*place(event))
+        start, size = span(half, part)
+        here = kv_ref.at[shard, pl.ds(start, size), :]
+        pltpu.make_async_copy(here, here, recv_sem.at[number]).wait()
+        pass_on(event, here)
+        to_partner(shard, start, size, here, number)
+    every = kv_ref.at[pl.ds(0, NZ * NY), :, :]
+    pltpu.make_async_copy(every, every, pair_recv.at[0]).wait()
+    keep.wait()
+    for copy in started:
+        copy.wait_send()
+
+
+def norm_rows(stream, gain, bias):
     center = jnp.mean(stream, axis=-1, keepdims=True)
     spread = jnp.mean(jnp.square(stream - center), axis=-1, keepdims=True)
-    return (stream - center) * lax.rsqrt(spread + eps_norm) * gain_vec + bias_vec
-
-
-def attend(queries, key_heads, value_heads, documents, query_gain, key_gain):
+    return (stream - center) * lax.rsqrt(spread + eps_norm) * gain + bias
+
+
+def expert_kernel(
+    att_ref, res_ref, routes_ref, weights_ref, ogain_ref, mgain_ref, mbias_ref, fgain_ref, fbias_ref,
+    proj_hbm, gate_hbm, up_hbm, down_hbm,
+    out_ref,
+    att_buf, proj, gate, up, down, stream, mid, sent, got, served, back, picked, xs,
+    load_sem, att_send, att_recv, go_send, go_recv, ret_send, ret_recv,
+):
+    sp, tp = lax.axis_index("sp"), lax.axis_index("tp")
+    core = sp % NC
+    y = (sp // NC) % NY
+    z = sp // (NC * NY)
+    tokens = res_ref.shape[0]
+    width = res_ref.shape[1]
+    chunks = width // WIDE
+    block = CAP * chunks
+    groups = 4
+    per_group = NZ * NY * NC * NX // groups
+    group_rows = per_group * block
+
+    loads = [
+        pltpu.make_async_copy(src, dst, load_sem.at[n])
+        for n, (src, dst) in enumerate(((proj_hbm, proj), (gate_hbm.at[0], gate), (up_hbm.at[0], up), (down_hbm.at[0], down)))
+    ]
+    for load in loads:
+        load.start()
+
+    def steps(g, r):
+        dx, dy, dc = r // (NY * NC), (r // NC) % NY, r % NC
+        return dx, dy, (g + 8 - dx - dy) % NZ, dc
+
+    def device_at(g, r, sign):
+        dx, dy, dz, dc = steps(g, r)
+        new_z = (z + NZ + sign * dz) % NZ
+        new_y = (y + NY + sign * dy) % NY
+        new_c = (core + dc) % NC
+        new_x = (tp + NX + sign * dx) % NX
+        return (new_z * (NY * NC) + new_y * NC + new_c, new_x)
+
+    barrier = pltpu.get_barrier_semaphore()
+    for g in range(groups):
+
+        @pl.loop(1 if g == 0 else 0, per_group)
+        def _(r, g=g):
+            pl.semaphore_signal(barrier, inc=1, device_id=device_at(g, r, 1), device_id_type=MESH)
+
+    named = routes_ref[...]
+    expert_lane = lax.broadcasted_iota(jnp.int32, (tokens, 128), 1)
+    hot = [(named[:, k : k + 1] == expert_lane).astype(jnp.float32) for k in (0, 1)]
+    earlier = (
+        lax.broadcasted_iota(jnp.int32, (tokens, tokens), 1) < lax.broadcasted_iota(jnp.int32, (tokens, tokens), 0)
+    ).astype(jnp.bfloat16)
+    counted = jnp.dot(earlier, (hot[0] + hot[1]).astype(jnp.bfloat16), preferred_element_type=jnp.float32)
+    slot_column, slot_row = [], []
+    for k in (0, 1):
+        rank = jnp.sum(hot[k] * counted, axis=1, keepdims=True).astype(jnp.int32)
+        e = named[:, k : k + 1]
+        dx = ((e & 3) + NX - tp) & 3
+        dc = (((e >> 2) & 1) + core) & 1
+        dy = (((e >> 3) & 3) + NY - y) & 3
+        dz = ((e >> 5) + NZ - z) & 3
+        place = ((dx + dy + dz) & 3) * per_group + dx * (NY * NC) + dy * NC + dc
+        column = place * block + rank
+        slot_column.append(column)
+        turned = jnp.transpose(jnp.broadcast_to(column.astype(jnp.float32), (tokens, 128)))
+        row = turned[0:1, :].astype(jnp.int32)
+        slot_row.append(jnp.concatenate([row + CAP * c for c in range(chunks)], axis=1))
+
+    pl.semaphore_wait(barrier, NZ * NY * NC * NX - 1)
+
+    copies = []
+    for j in range(1, NX):
+        to = (tp + j) % NX
+        copy = pltpu.make_async_remote_copy(
+            src_ref=att_ref.at[pl.ds(pl.multiple_of(to * tokens, tokens), tokens), :],
+            dst_ref=att_buf.at[j],
+            send_sem=att_send.at[j],
+            recv_sem=att_recv.at[j],
+            device_id=(sp, to),
+            device_id_type=MESH,
+        )
+        copy.start()
+        copies.append(copy)
+
+    loads[0].wait()
+    squares = jnp.zeros((tokens, 1), jnp.float32)
+    local = att_ref.shape[1]
+    for j in range(NX):
+        source = (tp + NX - j) % NX
+        if j == 0:
+            part = att_ref[pl.ds(pl.multiple_of(tp * tokens, tokens), tokens), :]
+        else:
+            copies[j - 1].wait_recv()
+            part = att_buf[j]
+        part = part.astype(jnp.float32)
+        squares = squares + jnp.sum(part * part, axis=1, keepdims=True)
+        scaled = (part * ogain_ref[pl.ds(source, 1), :]).astype(jnp.bfloat16)
+        product = jnp.dot(
+            scaled, proj[pl.ds(pl.multiple_of(source * local, local), local), :], preferred_element_type=jnp.float32
+        )
+        if j == 0:
+            stream[...] = product
+        else:
+            stream[...] += product
+    inv_rms = lax.rsqrt(squares / (NX * local) + eps_norm)
+
+    step_rows = 16
+    for n in range(tokens // step_rows):
+        part = slice(n * step_rows, (n + 1) * step_rows)
+        value = alpha_mix * res_ref[part, :].astype(jnp.float32) + stream[part, :] * inv_rms[part, :]
+        value = norm_rows(value, mgain_ref[...], mbias_ref[...]).astype(jnp.bfloat16)
+        for c in range(chunks):
+            mid[c * tokens + n * step_rows : c * tokens + (n + 1) * step_rows, :] = value[:, c * WIDE : (c + 1) * WIDE]
+
+    def row_iota(g):
+        return lax.broadcasted_iota(jnp.int32, (group_rows, chunks * tokens), 0) + g * group_rows
+
+    for g in range(groups):
+        rows = row_iota(g)
+        choose = ((rows == slot_row[0]) | (rows == slot_row[1])).astype(jnp.float32).astype(jnp.bfloat16)
+        sent[g * group_rows : (g + 1) * group_rows, :] = jnp.dot(
+            choose, mid[...], preferred_element_type=jnp.float32
+        ).astype(jnp.bfloat16)
+
+        @pl.loop(1 if g == 0 else 0, per_group)
+        def _(r, g=g):
+            at = pl.ds(pl.multiple_of((g * per_group + r) * block, block), block)
+            pltpu.make_async_remote_copy(
+                src_ref=sent.at[at, :],
+                dst_ref=got.at[at, :],
+                send_sem=go_send.at[g],
+                recv_sem=go_recv.at[g],
+                device_id=device_at(g, r, 1),
+                device_id_type=MESH,
+            ).start()
+
+    got[0:block, :] = sent[0:block, :]
+    for load in loads[1:]:
+        load.wait()
+
+    def whole(ref, g):
+        first = block if g == 0 else 0
+        return ref.at[pl.ds(g * group_rows + first, group_rows - first), :]
+
+    sub = 256
+    ii = lax.broadcasted_iota(jnp.int32, (sub, sub), 0)
+    jj = lax.broadcasted_iota(jnp.int32, (sub, sub), 1)
+    per_chunk = sub // chunks
+
+    def spot(i):
+        return ((i % per_chunk) // CAP) * block + (i // per_chunk) * CAP + i % CAP
+
+    collect = (jj == spot(ii)).astype(jnp.float32).astype(jnp.bfloat16)
+    scatter = (ii == spot(jj)).astype(jnp.float32).astype(jnp.bfloat16)
+    for g in range(groups):
+        pltpu.make_async_copy(whole(got, g), whole(got, g), go_recv.at[g]).wait()
+        for s in range(group_rows // sub):
+            ordered = jnp.dot(
+                collect, got[g * group_rows + s * sub : g * group_rows + (s + 1) * sub, :], preferred_element_type=jnp.float32
+            ).astype(jnp.bfloat16)
+            for c in range(chunks):
+                xs[s * per_chunk : (s + 1) * per_chunk, c * WIDE : (c + 1) * WIDE] = ordered[
+                    c * per_chunk : (c + 1) * per_chunk, :
+                ]
+        x = xs[...]
+        gate_part = jnp.dot(x, gate[...], preferred_element_type=jnp.float32)
+        up_part = jnp.dot(x, up[...], preferred_element_type=jnp.float32)
+        hidden = (gate_part / (1.0 + jnp.exp(-gate_part)) * up_part).astype(jnp.bfloat16)
+        result = jnp.dot(hidden, down[...], preferred_element_type=jnp.float32).astype(jnp.bfloat16)
+        for s in range(group_rows // sub):
+            stacked = jnp.concatenate(
+                [result[s * per_chunk : (s + 1) * per_chunk, c * WIDE : (c + 1) * WIDE] for c in range(chunks)], axis=0
+            )
+            served[g * group_rows + s * sub : g * group_rows + (s + 1) * sub, :] = jnp.dot(
+                scatter, stacked, preferred_element_type=jnp.float32
+            ).astype(jnp.bfloat16)
+
+        @pl.loop(1 if g == 0 else 0, per_group)
+        def _(r, g=g):
+            at = pl.ds(pl.multiple_of((g * per_group + r) * block, block), block)
+            pltpu.make_async_remote_copy(
+                src_ref=served.at[at, :],
+                dst_ref=back.at[at, :],
+                send_sem=ret_send.at[g],
+                recv_sem=ret_recv.at[g],
+                device_id=device_at(g, r, -1),
+                device_id_type=MESH,
+            ).start()
+
+    back[0:block, :] = served[0:block, :]
+
+    for g in range(groups):
+        pltpu.make_async_copy(whole(back, g), whole(back, g), ret_recv.at[g]).wait()
+        lanes = lax.broadcasted_iota(jnp.int32, (tokens, group_rows), 1) + g * group_rows
+        arrived = back[g * group_rows : (g + 1) * group_rows, :]
+        for c in range(chunks):
+            total = jnp.zeros((tokens, WIDE), jnp.float32)
+            for k in (0, 1):
+                choose = (lanes == slot_column[k] + CAP * c).astype(jnp.float32).astype(jnp.bfloat16)
+                total = total + weights_ref[:, k : k + 1] * jnp.dot(choose, arrived, preferred_element_type=jnp.float32)
+            if g == 0:
+                picked[:, c * WIDE : (c + 1) * WIDE] = total
+            else:
+                picked[:, c * WIDE : (c + 1) * WIDE] += total
+
+    for n in range(tokens // step_rows):
+        part = slice(n * step_rows, (n + 1) * step_rows)
+        value = jnp.concatenate(
+            [mid[c * tokens + n * step_rows : c * tokens + (n + 1) * step_rows, :] for c in range(chunks)], axis=1
+        )
+        value = alpha_mix * value.astype(jnp.float32) + picked[part, :]
+        out_ref[part, :] = norm_rows(value, fgain_ref[...], fbias_ref[...]).astype(jnp.bfloat16)
+
+    for copy in copies:
+        copy.wait_send()
+    for g in range(groups):
+        pltpu.make_async_copy(whole(sent, g), whole(sent, g), go_send.at[g]).wait()
+        pltpu.make_async_copy(whole(served, g), whole(served, g), ret_send.at[g]).wait()
+
+
+def per_device(
+    queries, key_heads, value_heads, documents, query_gain, key_gain, out_gain, out_proj, residual, mid_gain, mid_bias,
+    routes, route_weights, expert_gate, expert_up, expert_down, final_gain, final_bias,
+):
     rows = queries.shape[0]
     heads = queries.shape[1] // HEAD
-    shards = lax.axis_size("sp")
-    cosine, sine = rotary_tables(rows, lax.axis_index("sp") * rows)
+    shards = NZ * NY * NC
     docs = documents.reshape(2, rows // 2)
-    sent = pl.pallas_call(
-        key_kernel,
-        out_shape=jax.ShapeDtypeStruct((rows + 16, 2 * HEAD), jnp.bfloat16),
-        in_specs=[VMEM] * 6,
-        out_specs=VMEM,
-        cost_estimate=pl.CostEstimate(flops=1000000, bytes_accessed=1000000, transcendentals=0),
-        name="keys",
-    )(key_heads, value_heads, docs, key_gain.reshape(1, HEAD), cosine, sine)
-    filled = lax.all_gather(sent, "sp", axis=0, tiled=False)
-    query_rot = pl.pallas_call(
-        query_kernel,
-        out_shape=jax.ShapeDtypeStruct((heads, rows, HEAD), jnp.bfloat16),
-        in_specs=[VMEM] * 4,
-        out_specs=VMEM,
-        cost_estimate=pl.CostEstimate(flops=1000000, bytes_accessed=1000000, transcendentals=0),
-        name="queries",
-    )(queries, query_gain.reshape(1, HEAD), cosine, sine)
+    filled, query_rot = pl.pallas_call(
+        gather_kernel,
+        out_shape=(
+            jax.ShapeDtypeStruct((shards, rows + 16, 2 * HEAD), jnp.bfloat16),
+            jax.ShapeDtypeStruct((heads, rows, HEAD), jnp.bfloat16),
+        ),
+        in_specs=[VMEM] * 10,
+        out_specs=(ANY, VMEM),
+        scratch_shapes=[
+            pltpu.VMEM((rows + 16, 2 * HEAD), jnp.bfloat16),
+            pltpu.SemaphoreType.DMA((SEND_TOTAL,)),
+            pltpu.SemaphoreType.DMA((len(EVENTS),)),
+            pltpu.SemaphoreType.DMA((len(EVENTS) + 1,)),
+            pltpu.SemaphoreType.DMA((1,)),
+            pltpu.SemaphoreType.DMA((1,)),
+        ],
+        compiler_params=pltpu.CompilerParams(collective_id=0, has_side_effects=True),
+        name="gather",
+    )(
+        queries, key_heads, value_heads, docs, query_gain.reshape(1, HEAD), key_gain.reshape(1, HEAD),
+        *[jnp.asarray(t) for t in table_constants()],
+    )
     tile = rows // 2
-    return pl.pallas_call(
+    attention = pl.pallas_call(
         functools.partial(attention_kernel, shards, rows, tile),
         out_shape=jax.ShapeDtypeStruct((rows, heads * HEAD), jnp.bfloat16),
         in_specs=[VMEM, VMEM, ANY],
@@ -241,93 +594,47 @@
             pltpu.SemaphoreType.DMA((2 * shards + 1,)),
         ],
         compiler_params=pltpu.CompilerParams(vmem_limit_bytes=56 * 1024 * 1024),
-        cost_estimate=pl.CostEstimate(flops=6000000000, bytes_accessed=9000000, transcendentals=11000000),
         name="attention",
     )(query_rot, docs, filled)
-
-
-def per_device(
-    queries,
-    key_heads,
-    value_heads,
-    documents,
-    query_gain,
-    key_gain,
-    out_gain,
-    out_proj,
-    residual,
-    mid_gain,
-    mid_bias,
-    routes,
-    route_weights,
-    expert_gate,
-    expert_up,
-    expert_down,
-    final_gain,
-    final_bias,
-):
-    attention = attend(queries, key_heads, value_heads, documents, query_gain, key_gain)
-    tp_size = lax.axis_size("tp")
-    tiles = attention.reshape(tp_size, attention.shape[0] // tp_size, attention.shape[1])
-    arrived = lax.all_to_all(tiles, "tp", split_axis=0, concat_axis=0, tiled=True)
-    attention = jnp.transpose(arrived, (1, 0, 2)).reshape(arrived.shape[1], -1)
-    attn_float = attention.astype(jnp.float32)
-    mean_square = jnp.mean(attn_float * attn_float, axis=1, keepdims=True)
-    scaled = (attn_float * out_gain).astype(jnp.bfloat16)
-    projected = jnp.dot(scaled, out_proj, preferred_element_type=jnp.float32)
-    projected = projected * lax.rsqrt(mean_square + eps_norm)
-    middle = layer_norm(
-        alpha_mix * residual.astype(jnp.float32) + projected, mid_gain, mid_bias
-    ).astype(jnp.bfloat16)
-    out_rows = middle.shape[0]
-    model_width = middle.shape[1]
-    top_count = routes.shape[1]
-    local_experts = expert_gate.shape[0]
-    sp_size = lax.axis_size("sp")
-    tp_size = lax.axis_size("tp")
-    expert_total = local_experts * sp_size * tp_size
-    capacity = 2 * out_rows * top_count // expert_total
-    flat_routes = routes.reshape(-1)
-    one_hot = (flat_routes[:, None] == jnp.arange(expert_total, dtype=jnp.int32)[None, :]).astype(
-        jnp.int32
+    tokens, width = residual.shape
+    hidden = expert_gate.shape[2]
+    slots = NZ * NY * NC * NX * CAP * (width // WIDE)
+    vec = lambda v: v.reshape(1, -1)
+    return pl.pallas_call(
+        expert_kernel,
+        out_shape=jax.ShapeDtypeStruct((tokens, width), jnp.bfloat16),
+        in_specs=[VMEM] * 9 + [ANY] * 4,
+        out_specs=VMEM,
+        scratch_shapes=[
+            pltpu.VMEM((NX, tokens, heads * HEAD), jnp.bfloat16),
+            pltpu.VMEM(out_proj.shape, jnp.bfloat16),
+            pltpu.VMEM((width, hidden), jnp.bfloat16),
+            pltpu.VMEM((width, hidden), jnp.bfloat16),
+            pltpu.VMEM((hidden, width), jnp.bfloat16),
+            pltpu.VMEM((tokens, width), jnp.float32),
+            pltpu.VMEM((width // WIDE * tokens, WIDE), jnp.bfloat16),
+            pltpu.VMEM((slots, WIDE), jnp.bfloat16),
+            pltpu.VMEM((slots, WIDE), jnp.bfloat16),
+            pltpu.VMEM((slots, WIDE), jnp.bfloat16),
+            pltpu.VMEM((slots, WIDE), jnp.bfloat16),
+            pltpu.VMEM((tokens, width), jnp.float32),
+            pltpu.VMEM((tokens, width), jnp.bfloat16),
+            pltpu.SemaphoreType.DMA((4,)),
+            pltpu.SemaphoreType.DMA((NX,)),
+            pltpu.SemaphoreType.DMA((NX,)),
+            pltpu.SemaphoreType.DMA((4,)),
+            pltpu.SemaphoreType.DMA((4,)),
+            pltpu.SemaphoreType.DMA((4,)),
+            pltpu.SemaphoreType.DMA((4,)),
+        ],
+        compiler_params=pltpu.CompilerParams(
+            collective_id=1, has_side_effects=True, vmem_limit_bytes=56 * 1024 * 1024
+        ),
+        name="experts",
+    )(
+        attention, residual, routes, route_weights, out_gain.reshape(NX, -1), vec(mid_gain), vec(mid_bias),
+        vec(final_gain), vec(final_bias), out_proj, expert_gate, expert_up, expert_down,
     )
-    rank_in = jnp.sum((jnp.cumsum(one_hot, axis=0) - one_hot) * one_hot, axis=1)
-    target = flat_routes * capacity + rank_in
-    outbound = (
-        jnp.zeros((expert_total * capacity, model_width), jnp.bfloat16)
-        .at[target]
-        .set(jnp.repeat(middle, top_count, axis=0))
-    )
-    arrived = lax.all_to_all(
-        outbound.reshape(expert_total, capacity, model_width),
-        ("sp", "tp"),
-        split_axis=0,
-        concat_axis=0,
-        tiled=True,
-    )
-    item_count = arrived.shape[-2]
-    grouped_rows = arrived.reshape(-1, local_experts, item_count, model_width)
-    gate_part = jnp.einsum(
-        "sekd,edf->sekf", grouped_rows, expert_gate, preferred_element_type=jnp.float32
-    )
-    up_part = jnp.einsum(
-        "sekd,edf->sekf", grouped_rows, expert_up, preferred_element_type=jnp.float32
-    )
-    hidden = (jax.nn.silu(gate_part) * up_part).astype(jnp.bfloat16)
-    served = jnp.einsum("sekf,efd->sekd", hidden, expert_down, preferred_element_type=jnp.float32)
-    returned = lax.all_to_all(
-        served.astype(jnp.bfloat16).reshape(arrived.shape),
-        ("sp", "tp"),
-        split_axis=0,
-        concat_axis=0,
-        tiled=True,
-    )
-    picked = returned.reshape(expert_total * capacity, model_width)[target]
-    picked = picked.astype(jnp.float32).reshape(out_rows, top_count, model_width)
-    routed = jnp.sum(picked * route_weights[:, :, None], axis=1)
-    return layer_norm(
-        alpha_mix * middle.astype(jnp.float32) + routed, final_gain, final_bias
-    ).astype(jnp.bfloat16)
 
 
 def solution(mesh):

time: 252 us -> 163 us (0.65)
  the two profiles are of different devices: /device:TPU:1 before, /device:TPU:2 now
where the time goes in v2:
time: 163 us; the launch traced here: 164 us
  Pallas kernels  159 us (98%)
  local copies, waits for them, and re-layouts  5.23 us (3%)
    pallas_call x1, Pallas kernels, per_device(): pl.pallas_call(expert_kernel, out_shape=jax.ShapeDtypeStruct((tokens, wid...  110 us
    pallas_call x1, Pallas kernels, per_device(): pl.pallas_call(gather_kernel, out_shape=(jax.ShapeDtypeStruct((shards, ro...  36.7 us
    pallas_call x1, Pallas kernels, per_device(): pl.pallas_call(functools.partial(attention_kernel, shards, rows, tile), o...  12.5 us
    unnamed x9, local copies, waits for them, and re-layouts  3.36 us

profile of v2, /device:TPU:2, one launch (start us, length us, event | category | flops | bytes accessed | tf_op | source)
XLA Modules:
  0.0 164.3 jit_solution(17417327541268082287)
XLA Ops:
  0.0 1.3 reshape.24.docs_ref
  1.3 36.7 %gather.1 = (bf16[32,528,256]{2,1,0:T(8,128)(2,1)}, bf16[2,512,128]{2,1,0:T(8,128)(2,1)}) custom-call(bf16[512,256]{1,0:T(8,128)(2,1)} %query_ref.1, bf16[512,128]{1,0:T(8,128)(2,1)} %key_ref.1, bf16[512,128]{1,0:T(8,128)(2,1)} %value_ref.1, s32[2,256]{1,0:T(2,128)} %reshape.24.docs_ref, f32[1,128]{1,0:T(1,128)} %bitcast.10, f32[1,128]{1,0:T(1,128)} %bitcast.11, ...), custom_call_target="tpu_custom_call" | custom-call | tf_op jit(solution)/shard_map/gather/pallas_call | solution.py:558
  38.0 0.0 copy-start.1
  38.0 0.0 copy-start.2
  38.0 0.0 copy-start
  38.0 12.5 %attention.1.att_ref = bf16[512,256]{1,0:T(8,128)(2,1)} custom-call(bf16[2,512,128]{2,1,0:T(8,128)(2,1)} %get-tuple-element.7.q_ref, s32[2,256]{1,0:T(2,128)} %reshape.24.docs_ref, bf16[32,528,256]{2,1,0:T(8,128)(2,1)} %get-tuple-element.8.kv_ref), custom_call_target="tpu_custom_call" | custom-call | tf_op jit(solution)/shard_map/attention/pallas_call | solution.py:581
  50.5 0.0 copy-done.1
  50.5 0.7 copy.23.routes_ref
  51.2 0.0 copy-done.2
  51.2 0.7 copy.24.weights_ref
  51.9 0.0 copy-done
  51.9 0.6 reshape.27.ogain_ref
  52.5 109.8 %experts.1 = bf16[128,2048]{1,0:T(8,128)(2,1)} custom-call(bf16[512,256]{1,0:T(8,128)(2,1)} %attention.1.att_ref, bf16[128,2048]{1,0:T(8,128)(2,1)} %res_ref.1, s32[128,2]{1,0:T(8,128)} %copy.23.routes_ref, f32[128,2]{1,0:T(8,128)} %copy.24.weights_ref, f32[4,256]{1,0:T(4,128)} %reshape.27.ogain_ref, f32[1,2048]{1,0:T(1,128)} %bitcast.6, f32[1,2048]{1,0:T(1,128)} %bitcast.7, ...), custom_call_target="tpu_custom_call" | custom-call | tf_op jit(solution)/shard_map/experts/pallas_call | solution.py:603
  162.4 1.9 %copy.26 = bf16[128,2048]{1,0:T(8,128)(2,1)} copy(bf16[128,2048]{1,0:T(8,128)(2,1)} %experts.1) | data formatting | bytes 1048576
Async XLA Ops:
  38.0 12.5 %copy-start.1 = (s32[128,2]{0,1:T(2,128)S(1)}, s32[128,2]{0,1:T(2,128)}, u32[]{:S(2)}) copy-start(s32[128,2]{0,1:T(2,128)} %param.33) | copy-start | bytes 3076
  38.0 13.2 %copy-start.2 = (f32[128,2]{0,1:T(2,128)S(1)}, f32[128,2]{0,1:T(2,128)}, u32[]{:S(2)}) copy-start(f32[128,2]{0,1:T(2,128)} %param.34) | copy-start | bytes 3076
  38.0 14.0 %copy-start = (f32[1024]{0:T(1024)S(1)}, f32[1024]{0:T(1024)}, u32[]{:S(2)}) copy-start(f32[1024]{0:T(1024)} %param.28) | copy-start | bytes 12292

commit v3 on v2

--- a/solution.py
+++ b/solution.py
@@ -11,8 +11,6 @@
 
 HEAD = 128
 GRID = 64
-KEY_BLOCK = 1152
-ALIGN = 128
 
 eps_norm = 1e-06
 alpha_mix = 8.0**0.25
@@ -28,136 +26,6 @@
     values = values * inv_rms * gain
     swapped = pltpu.roll(values, HEAD // 2, 1)
     return (values * cosine + swapped * sine).astype(jnp.bfloat16)
-
-
-def attention_kernel(shards, rows, tile, q_ref, docs_ref, kv_ref, out_ref, k_buf, v_buf, d_buf, start_buf, end_buf, acc, top, sem):
-    heads = q_ref.shape[0]
-    total_keys = shards * rows
-    doc_copy = pltpu.make_async_copy(kv_ref.at[:, pl.ds(rows, 16), :], d_buf, sem.at[2 * shards])
-    doc_copy.start()
-    v_buf[:, HEAD:] = jnp.ones((v_buf.shape[0], HEAD), jnp.bfloat16)
-    v_buf[total_keys:, 0:HEAD] = jnp.zeros((KEY_BLOCK, HEAD), jnp.bfloat16)
-    doc_copy.wait()
-    all_docs = d_buf[:, 0:8, :].astype(jnp.float32).astype(jnp.int32)[:, 0:2, :]
-    docs_here = docs_ref[...]
-    half = rows // 2
-
-    counts = [
-        jnp.sum(jnp.sum((all_docs < d).astype(jnp.float32), axis=(0, 1), keepdims=False)[None, :], axis=1, keepdims=True)
-        for d in range(1, 9)
-    ]
-    counts = [jnp.zeros((1, 1), jnp.float32)] + counts + [jnp.full((1, 1), float(total_keys), jnp.float32)]
-    bounds = []
-    for t in range(rows // tile):
-        per_row = half // tile
-        mine = docs_here[t // per_row : t // per_row + 1, (t % per_row) * tile : (t % per_row + 1) * tile]
-        start_row = jnp.zeros(mine.shape, jnp.float32)
-        end_row = jnp.zeros(mine.shape, jnp.float32)
-        for d in range(9):
-            start_row = jnp.where(mine == d, counts[d], start_row)
-            end_row = jnp.where(mine == d, counts[d + 1], end_row)
-        for row, buf in ((start_row, start_buf), (end_row, end_buf)):
-            column = jnp.transpose(jnp.broadcast_to(row, (HEAD, tile))).astype(jnp.int32)
-            buf[t * tile : (t + 1) * tile, :] = column
-        start, last_start = jnp.min(start_row).astype(jnp.int32), jnp.max(start_row).astype(jnp.int32)
-        bounds.append((start, jnp.max(end_row).astype(jnp.int32), start == last_start))
-
-    def base_of(t):
-        return (bounds[t][0] // ALIGN) * ALIGN
-
-    def blocks_of(t):
-        return (bounds[t][1] - base_of(t) + KEY_BLOCK - 1) // KEY_BLOCK
-
-    first_shard = base_of(0) // rows
-    limit = base_of(0)
-    for t in range(rows // tile):
-        limit = jnp.maximum(limit, base_of(t) + blocks_of(t) * KEY_BLOCK)
-    last_shard = jnp.minimum((limit + rows - 1) // rows, shards)
-
-    def k_copy(s):
-        return pltpu.make_async_copy(
-            kv_ref.at[s, pl.ds(0, rows), pl.ds(0, HEAD)],
-            k_buf.at[pl.ds(pl.multiple_of(s * rows, rows), rows), :],
-            sem.at[s],
-        )
-
-    def v_copy(s):
-        return pltpu.make_async_copy(
-            kv_ref.at[s, pl.ds(0, rows), pl.ds(HEAD, HEAD)],
-            v_buf.at[pl.ds(pl.multiple_of(s * rows, rows), rows), pl.ds(0, HEAD)],
-            sem.at[shards + s],
-        )
-
-    @pl.loop(first_shard, last_shard)
-    def _(s):
-        k_copy(s).start()
-        v_copy(s).start()
-
-    waited = first_shard
-    for t in range(rows // tile):
-        base = base_of(t)
-        q = q_ref[:, t * tile : (t + 1) * tile, :].reshape(heads * tile, HEAD)
-        acc[...] = jnp.zeros_like(acc)
-        top[...] = jnp.full_like(top, -1e30)
-        start, end, single = bounds[t]
-
-        def advance(q, offset, masked, t=t):
-            offset = pl.multiple_of(offset, ALIGN)
-            keys = k_buf[pl.ds(offset, KEY_BLOCK), :]
-            values = v_buf[pl.ds(offset, KEY_BLOCK), :]
-            scores = lax.dot_general(q, keys, (((1,), (1,)), ((), ())), preferred_element_type=jnp.float32)
-            if masked:
-                place = offset + lax.broadcasted_iota(jnp.int32, (heads * tile, KEY_BLOCK), 1)
-                reps = KEY_BLOCK // HEAD
-
-                def spread(buf):
-                    one = buf[t * tile : (t + 1) * tile, :]
-                    both = jnp.concatenate([one] * heads, axis=0)
-                    return jnp.concatenate([both] * reps, axis=1)
-
-                allowed = (place >= spread(start_buf)) & (place < spread(end_buf))
-                scores = jnp.where(allowed, scores, -1e30)
-            old = top[...]
-            new = jnp.maximum(old, jnp.max(scores, axis=1, keepdims=True))
-            shift = jnp.concatenate([new * LOG2_SCALE] * (KEY_BLOCK // HEAD), axis=1)
-            weights = jnp.exp2(scores * LOG2_SCALE - shift)
-            if masked:
-                weights = jnp.where(allowed, weights, 0.0)
-            rescale = jnp.exp2((old - new) * LOG2_SCALE)
-            part = jnp.dot(weights.astype(jnp.bfloat16), values, preferred_element_type=jnp.float32)
-            acc[...] = acc[...] * jnp.concatenate([rescale, rescale], axis=1) + part
-            top[...] = new
-
-        def step(b, waited):
-            offset = base + b * KEY_BLOCK
-            need = jnp.minimum((offset + KEY_BLOCK + rows - 1) // rows, shards)
-
-            @pl.loop(waited, need)
-            def _(s):
-                k_copy(s).wait()
-                v_copy(s).wait()
-
-            inside = single & (offset >= start) & (offset + KEY_BLOCK <= end)
-
-            @pl.when(inside)
-            def _():
-                advance(q, offset, False)
-
-            @pl.when(jnp.logical_not(inside))
-            def _():
-                advance(q, offset, True)
-
-            return jnp.maximum(waited, need)
-
-        waited = lax.fori_loop(0, blocks_of(t), step, waited)
-        result = (acc[:, 0:HEAD] / acc[:, HEAD:]).astype(jnp.bfloat16)
-        for head in range(heads):
-            out_ref[t * tile : (t + 1) * tile, head * HEAD : (head + 1) * HEAD] = result[head * tile : (head + 1) * tile]
-
-    @pl.loop(waited, last_shard)
-    def _(s):
-        k_copy(s).wait()
-        v_copy(s).wait()
 
 
 NZ, NY, NC, NX = 4, 4, 2, 4
@@ -181,13 +49,14 @@
     return tables
 
 
-PIECES = ((0, 128), (128, 128), (256, 128), (384, 144))
-
-
-def span(half, part):
-    if part is None:
-        return PIECES[2 * half][0], PIECES[2 * half][1] + PIECES[2 * half + 1][1]
-    return PIECES[2 * half + part]
+DOC_ROWS = 16
+HALF_ROWS = HEAD + DOC_ROWS + HEAD
+PART_ROWS = ((0, HEAD + DOC_ROWS), (HEAD + DOC_ROWS, HEAD))
+SAME_DOC = 32768.0
+
+
+def span(part):
+    return (0, HALF_ROWS) if part is None else PART_ROWS[part]
 
 
 def gather_events():
@@ -204,6 +73,9 @@
 
 EVENTS = gather_events()
 EVENT_ID = {e: n for n, e in enumerate(EVENTS)}
+UNITS = [(0, (0, 0)), (1, (0, 0)), (0, (0, -1)), (0, (0, 1)), (0, (-1, 0)), (0, (1, 0)), (1, (-1, 0)), (1, (1, 0)), (1, (0, -1)), (1, (0, 1)), (0, (0, 2)), (0, (-1, -1)), (0, (1, -1)), (1, (-1, -1)), (1, (-1, 1)), (0, (-1, 1)), (0, (1, 1)), (0, (2, 0)), (1, (1, -1)), (1, (1, 1)), (1, (2, 0)), (1, (0, 2)), (1, (-1, 2)), (0, (1, 2)), (0, (-1, 2)), (1, (1, 2)), (0, (2, -1)), (1, (2, 1)), (0, (2, 1)), (1, (2, -1)), (0, (2, 2)), (1, (2, 2))]
+GAPS = [[], [0, 1, 2, 3], [4, 5, 6, 7], [9, 8], [16, 17], [20, 21, 18, 19], [11, 10, 22, 23], [13, 12, 15, 14], [27, 26, 37, 36, 25, 39, 24], [38, 29, 35, 28, 34], [31, 33, 30, 32, 42], [40, 43], [41], [], [], []]
+UNIT_ID = {unit: n for n, unit in enumerate(UNITS)}
 
 
 def sends_of(event):
@@ -225,101 +97,149 @@
     return out
 
 
-SEND_TOTAL = sum(len(sends_of(e)) for e in EVENTS + [(0, 0, 0, None), (1, 0, 0, None)])
-
-
-def gather_kernel(
+def unit_of(event):
+    half, i, j, part = event
+    wrap = lambda v: (v + 1) % 4 - 1
+    return UNIT_ID[(half, (wrap(-i), wrap(-j)) if half == 0 else (wrap(-j), wrap(-i)))]
+
+
+OWN = ((0, 0, 0, None), (1, 0, 0, None))
+SENDS = [(e, axis, step, target) for e in list(OWN) + EVENTS for axis, step, target in sends_of(e)]
+
+
+def attention_kernel(
     query_ref, key_ref, value_ref, docs_ref, qgain_ref, kgain_ref, rowc_ref, rows_ref, colc_ref, cols_ref,
-    kv_ref, q_ref, own, send_sem, recv_sem, pair_send, pair_recv, local_sem,
+    out_ref,
+    slots, queries, acc, top, low, send_sem, recv_sem, pair_send, pair_recv,
 ):
     sp, tp = lax.axis_index("sp"), lax.axis_index("tp")
     core = sp % NC
     y = (sp // NC) % NY
     z = sp // (NC * NY)
     rows = key_ref.shape[0]
-
-    def shard_at(dz, dy):
-        return ((z + dz + 2 * NZ) % NZ) * (NY * NC) + ((y + dy + 2 * NY) % NY) * NC + core
-
+    half_rows = rows // 2
+    heads = query_ref.shape[1] // HEAD
     partner = sp + 1 - 2 * core
+    near = {}
+    for step in (1, -1):
+        near[True, step] = z * (NY * NC) + ((y + NY + step) % NY) * NC + core
+        near[False, step] = ((z + NZ + step) % NZ) * (NY * NC) + y * NC + core
+
     barrier = pltpu.get_barrier_semaphore()
-    for dz, dy in ((0, 1), (0, -1), (1, 0), (-1, 0)):
-        pl.semaphore_signal(barrier, inc=1, device_id=(shard_at(dz, dy), tp), device_id_type=MESH)
-    pl.semaphore_signal(barrier, inc=1, device_id=(partner, tp), device_id_type=MESH)
+    for to in list(near.values()) + [partner]:
+        pl.semaphore_signal(barrier, inc=1, device_id=(to, tp), device_id_type=MESH)
 
     def table(row_ref, col_ref):
-        near = row_ref[pl.ds(pl.multiple_of(sp * 8, 8), 8), :]
-        return jnp.concatenate([col_ref[...] + near[n : n + 1, :] for n in range(8)], axis=0)
+        mine = row_ref[pl.ds(pl.multiple_of(sp * 8, 8), 8), :]
+        return jnp.concatenate([col_ref[...] + mine[n : n + 1, :] for n in range(8)], axis=0)
 
     cosine, sine = table(rowc_ref, colc_ref), table(rows_ref, cols_ref)
-    own[0:rows, 0:HEAD] = turn(key_ref[...].astype(jnp.float32), kgain_ref[...], cosine, sine)
-    own[0:rows, HEAD:] = value_ref[...]
-    docs = docs_ref[...].astype(jnp.float32)
-    padded = jnp.concatenate([docs, jnp.zeros((16 - docs.shape[0], docs.shape[1]), jnp.float32)], axis=0)
-    own[rows:, :] = padded.astype(jnp.bfloat16)
+    turned = turn(key_ref[...].astype(jnp.float32), kgain_ref[...], cosine, sine).astype(jnp.float32)
+    numbers = lax.broadcasted_iota(jnp.int32, (HEAD, half_rows), 0)
+    for h in range(2):
+        part = slice(h * half_rows, (h + 1) * half_rows)
+        unit = unit_of(OWN[h])
+        slots[unit, 0, 0:HEAD, :] = jnp.transpose(turned[part, :]).astype(jnp.bfloat16)
+        same = (numbers[0:DOC_ROWS, :] == docs_ref[h : h + 1, :]).astype(jnp.float32)
+        slots[unit, 0, HEAD : HEAD + DOC_ROWS, :] = same.astype(jnp.bfloat16)
+        for k in range(2):
+            slots[unit, 0, HEAD + DOC_ROWS :, k * HEAD : (k + 1) * HEAD] = value_ref[
+                h * half_rows + k * HEAD : h * half_rows + (k + 1) * HEAD, :
+            ]
     pl.semaphore_wait(barrier, 5)
 
-    started = []
-    counter = [0]
-
-    def place(event):
-        half, i, j, part = event
-        return (-i, -j) if half == 0 else (-j, -i)
-
-    def pass_on(event, source):
-        for axis, step, target in sends_of(event):
-            half, i, j, part = target
-            along_y = (axis == 0) == (half == 0)
-            start, size = span(half, part)
-            shard = shard_at(*place(event))
-            dst = kv_ref.at[shard, pl.ds(start, size), :]
-            src = own.at[pl.ds(start, size), :] if source is None else dst
-            copy = pltpu.make_async_remote_copy(
-                src_ref=src,
-                dst_ref=dst,
-                send_sem=send_sem.at[counter[0]],
-                recv_sem=recv_sem.at[EVENT_ID[target]],
-                device_id=(shard_at(0, step) if along_y else shard_at(step, 0), tp),
-                device_id_type=MESH,
-            )
-            counter[0] += 1
-            copy.start()
-            started.append(copy)
-
-    def to_partner(shard, start, size, src, number):
-        copy = pltpu.make_async_remote_copy(
-            src_ref=src,
-            dst_ref=kv_ref.at[shard, pl.ds(start, size), :],
+    def sent_copy(number):
+        event, axis, step, target = SENDS[number]
+        half = event[0]
+        start, size = span(target[3])
+        return pltpu.make_async_remote_copy(
+            src_ref=slots.at[unit_of(event), 0, pl.ds(start, size), :],
+            dst_ref=slots.at[unit_of(target), 0, pl.ds(start, size), :],
+            send_sem=send_sem.at[number],
+            recv_sem=recv_sem.at[EVENT_ID[target]],
+            device_id=(near[(axis == 0) == (half == 0), step], tp),
+            device_id_type=MESH,
+        )
+
+    def pair_copy(event, number):
+        start, size = span(event[3])
+        return pltpu.make_async_remote_copy(
+            src_ref=slots.at[unit_of(event), 0, pl.ds(start, size), :],
+            dst_ref=slots.at[unit_of(event), 1, pl.ds(start, size), :],
             send_sem=pair_send.at[number],
-            recv_sem=pair_recv.at[0],
+            recv_sem=pair_recv.at[unit_of(event)],
             device_id=(partner, tp),
             device_id_type=MESH,
         )
-        copy.start()
-        started.append(copy)
-
-    for half in (0, 1):
-        pass_on((half, 0, 0, None), None)
-    to_partner(sp, 0, rows + 16, own, len(EVENTS))
-    keep = pltpu.make_async_copy(own, kv_ref.at[sp], local_sem.at[0])
-    keep.start()
-    for head in range(q_ref.shape[0]):
-        q_ref[head] = turn(
+
+    def pass_on(event):
+        for number, entry in enumerate(SENDS):
+            if entry[0] == event:
+                sent_copy(number).start()
+        pair_copy(event, (list(OWN) + EVENTS).index(event)).start()
+
+    for event in OWN:
+        pass_on(event)
+
+    columns = [jnp.transpose((numbers == docs_ref[h : h + 1, :]).astype(jnp.float32)) for h in range(2)]
+    same = (jnp.concatenate(columns, axis=0) * SAME_DOC).astype(jnp.bfloat16)
+    for head in range(heads):
+        queries[head, :, 0:HEAD] = turn(
             query_ref[:, head * HEAD : (head + 1) * HEAD].astype(jnp.float32), qgain_ref[...], cosine, sine
         )
-    for number, event in enumerate(EVENTS):
-        half, i, j, part = event
-        shard = shard_at(*place(event))
-        start, size = span(half, part)
-        here = kv_ref.at[shard, pl.ds(start, size), :]
-        pltpu.make_async_copy(here, here, recv_sem.at[number]).wait()
-        pass_on(event, here)
-        to_partner(shard, start, size, here, number)
-    every = kv_ref.at[pl.ds(0, NZ * NY), :, :]
-    pltpu.make_async_copy(every, every, pair_recv.at[0]).wait()
-    keep.wait()
-    for copy in started:
-        copy.wait_send()
+        queries[head, :, HEAD:] = same[:, 0:DOC_ROWS]
+    acc[...] = jnp.zeros_like(acc)
+    low[...] = jnp.zeros_like(low)
+    top[...] = jnp.full_like(top, -1e20)
+
+    def advance(k):
+        places = [(2 * k + n, c) for n in range(2) for c in range(2)]
+        keys = jnp.concatenate([slots[u, c, 0 : HEAD + DOC_ROWS, :] for u, c in places], axis=1)
+        values = jnp.concatenate(
+            [slots[u, c, HEAD + DOC_ROWS :, n * HEAD : (n + 1) * HEAD] for u, c in places for n in range(2)], axis=0
+        )
+        lanes = keys.shape[1] // HEAD
+        scores = [jnp.dot(queries[h], keys, preferred_element_type=jnp.float32) for h in range(heads)]
+        for h in range(heads):
+            old = top[h]
+            new = jnp.maximum(old, jnp.max(scores[h], axis=1, keepdims=True))
+            rescale = jnp.exp2((old - new) * LOG2_SCALE)
+            weights = jnp.exp2((scores[h] - jnp.concatenate([new] * lanes, axis=1)) * LOG2_SCALE)
+            sums = weights[:, 0:HEAD]
+            for n in range(1, lanes):
+                sums = sums + weights[:, n * HEAD : (n + 1) * HEAD]
+            low[h] = low[h] * rescale + sums
+            top[h] = new
+            acc[h] = acc[h] * rescale + jnp.dot(
+                weights.astype(jnp.bfloat16), values, preferred_element_type=jnp.float32
+            )
+
+    def step(k, carry):
+        for n, gap in enumerate(GAPS):
+
+            @pl.when(k == n)
+            def _(n=n, gap=gap):
+                for number in gap:
+                    event = EVENTS[number]
+                    start, size = span(event[3])
+                    here = slots.at[unit_of(event), 0, pl.ds(start, size), :]
+                    pltpu.make_async_copy(here, here, recv_sem.at[number]).wait()
+                    pass_on(event)
+                for unit in (2 * n, 2 * n + 1):
+                    here = slots.at[unit, 1, :, :]
+                    pltpu.make_async_copy(here, here, pair_recv.at[unit]).wait()
+
+        advance(k)
+        return carry
+
+    lax.fori_loop(0, len(GAPS), step, 0)
+    for h in range(heads):
+        total = jnp.sum(low[h], axis=1, keepdims=True)
+        out_ref[:, h * HEAD : (h + 1) * HEAD] = (acc[h] / total).astype(jnp.bfloat16)
+    for number in range(len(SENDS)):
+        sent_copy(number).wait_send()
+    for number, event in enumerate(list(OWN) + EVENTS):
+        pair_copy(event, number).wait_send()
 
 
 def norm_rows(stream, gain, bias):
@@ -553,49 +473,31 @@
 ):
     rows = queries.shape[0]
     heads = queries.shape[1] // HEAD
-    shards = NZ * NY * NC
     docs = documents.reshape(2, rows // 2)
-    filled, query_rot = pl.pallas_call(
-        gather_kernel,
-        out_shape=(
-            jax.ShapeDtypeStruct((shards, rows + 16, 2 * HEAD), jnp.bfloat16),
-            jax.ShapeDtypeStruct((heads, rows, HEAD), jnp.bfloat16),
+    attention = pl.pallas_call(
+        attention_kernel,
+        out_shape=jax.ShapeDtypeStruct((rows, heads * HEAD), jnp.bfloat16),
+        in_specs=[VMEM] * 10,
+        out_specs=VMEM,
+        scratch_shapes=[
+            pltpu.VMEM((len(UNITS), NC, HALF_ROWS, 2 * HEAD), jnp.bfloat16),
+            pltpu.VMEM((heads, rows, HEAD + DOC_ROWS), jnp.bfloat16),
+            pltpu.VMEM((heads, rows, HEAD), jnp.float32),
+            pltpu.VMEM((heads, rows, HEAD), jnp.float32),
+            pltpu.VMEM((heads, rows, HEAD), jnp.float32),
+            pltpu.SemaphoreType.DMA((len(SENDS),)),
+            pltpu.SemaphoreType.DMA((len(EVENTS),)),
+            pltpu.SemaphoreType.DMA((len(EVENTS) + 2,)),
+            pltpu.SemaphoreType.DMA((len(UNITS),)),
+        ],
+        compiler_params=pltpu.CompilerParams(
+            collective_id=0, has_side_effects=True, vmem_limit_bytes=48 * 1024 * 1024
         ),
-        in_specs=[VMEM] * 10,
-        out_specs=(ANY, VMEM),
-        scratch_shapes=[
-            pltpu.VMEM((rows + 16, 2 * HEAD), jnp.bfloat16),
-            pltpu.SemaphoreType.DMA((SEND_TOTAL,)),
-            pltpu.SemaphoreType.DMA((len(EVENTS),)),
-            pltpu.SemaphoreType.DMA((len(EVENTS) + 1,)),
-            pltpu.SemaphoreType.DMA((1,)),
-            pltpu.SemaphoreType.DMA((1,)),
-        ],
-        compiler_params=pltpu.CompilerParams(collective_id=0, has_side_effects=True),
-        name="gather",
+        name="attention",
     )(
         queries, key_heads, value_heads, docs, query_gain.reshape(1, HEAD), key_gain.reshape(1, HEAD),
         *[jnp.asarray(t) for t in table_constants()],
     )
-    tile = rows // 2
-    attention = pl.pallas_call(
-        functools.partial(attention_kernel, shards, rows, tile),
-        out_shape=jax.ShapeDtypeStruct((rows, heads * HEAD), jnp.bfloat16),
-        in_specs=[VMEM, VMEM, ANY],
-        out_specs=VMEM,
-        scratch_shapes=[
-            pltpu.VMEM((shards * rows + KEY_BLOCK, HEAD), jnp.bfloat16),
-            pltpu.VMEM((shards * rows + KEY_BLOCK, 2 * HEAD), jnp.bfloat16),
-            pltpu.VMEM((shards, 16, 2 * HEAD), jnp.bfloat16),
-            pltpu.VMEM((rows, HEAD), jnp.int32),
-            pltpu.VMEM((rows, HEAD), jnp.int32),
-            pltpu.VMEM((heads * tile, 2 * HEAD), jnp.float32),
-            pltpu.VMEM((heads * tile, HEAD), jnp.float32),
-            pltpu.SemaphoreType.DMA((2 * shards + 1,)),
-        ],
-        compiler_params=pltpu.CompilerParams(vmem_limit_bytes=56 * 1024 * 1024),
-        name="attention",
-    )(query_rot, docs, filled)
     tokens, width = residual.shape
     hidden = expert_gate.shape[2]
     slots = NZ * NY * NC * NX * CAP * (width // WIDE)

time: 163 us -> 134 us (0.82)
  the two profiles are of different devices: /device:TPU:2 before, /device:TPU:1 now
where the time goes in v3:
time: 134 us; the launch traced here: 133 us
  Pallas kernels  118 us (88%)
  local copies, waits for them, and re-layouts  14.7 us (11%)
    pallas_call x1, Pallas kernels, per_device(): pl.pallas_call(expert_kernel, out_shape=jax.ShapeDtypeStruct((tokens, wid...  75.3 us
    pallas_call x1, Pallas kernels, per_device(): pl.pallas_call(attention_kernel, out_shape=jax.ShapeDtypeStruct((rows, he...  43 us
    unnamed x23, local copies, waits for them, and re-layouts  12.8 us

profile of v3, /device:TPU:1, one launch (start us, length us, event | category | flops | bytes accessed | tf_op | source)
XLA Modules:
  0.0 133.2 jit_solution(11407896769768836100)
XLA Ops:
  0.0 0.7 reshape.24.docs_ref
  0.7 1.3 reshape.27.ogain_ref
  2.0 1.4 %copy.23.routes_ref = s32[128,2]{1,0:T(8,128)} copy(s32[128,2]{0,1:T(2,128)} %param.33) | data formatting | bytes 2048 | tf_op args[11]
  3.4 1.4 %copy.24.weights_ref = f32[128,2]{1,0:T(8,128)} copy(f32[128,2]{0,1:T(2,128)} %param.34) | data formatting | bytes 2048 | tf_op args[12]
  4.8 0.0 copy-start.1
  4.8 0.9 copy-done.1
  5.7 0.0 copy-start.2
  5.7 0.9 copy-done.2
  6.6 0.0 copy-start.3
  6.6 0.9 copy-done.3
  7.5 0.0 copy-start.4
  7.5 0.9 copy-done.4
  8.4 0.0 copy-start.5
  8.4 0.9 copy-done.5
  9.4 0.0 copy-start.6
  9.4 0.8 copy-done.6
  10.1 0.0 copy-start.7
  10.1 0.8 copy-done.7
  10.9 0.0 copy-start.8
  10.9 0.7 copy-done.8
  11.5 0.0 copy-start.9
  11.5 0.7 copy-done.9
  12.2 43.0 %attention.1.att_ref = bf16[512,256]{1,0:T(8,128)(2,1)S(1)} custom-call(bf16[512,256]{1,0:T(8,128)(2,1)S(1)} %copy-done.1, bf16[512,128]{1,0:T(8,128)(2,1)S(1)} %copy-done.2, bf16[512,128]{1,0:T(8,128)(2,1)S(1)} %copy-done.3, s32[2,256]{1,0:T(2,128)S(1)} %reshape.24.docs_ref, f32[1,128]{1,0:T(1,128)S(1)} %bitcast.6, f32[1,128]{1,0:T(1,128)S(1)} %bitcast.7, ...), custom_call_target="tpu_custom_call" | custom-call | tf_op jit(solution)/shard_map/attention/pallas_call | solution.py:477
  55.2 0.0 copy-start
  55.2 0.7 copy-done
  55.9 75.3 %experts.1 = bf16[128,2048]{1,0:T(8,128)(2,1)} custom-call(bf16[512,256]{1,0:T(8,128)(2,1)} %copy-done, bf16[128,2048]{1,0:T(8,128)(2,1)} %res_ref.1, s32[128,2]{1,0:T(8,128)} %copy.23.routes_ref, f32[128,2]{1,0:T(8,128)} %copy.24.weights_ref, f32[4,256]{1,0:T(4,128)} %reshape.27.ogain_ref, f32[1,2048]{1,0:T(1,128)} %bitcast.8, f32[1,2048]{1,0:T(1,128)} %bitcast.9, ...), custom_call_target="tpu_custom_call" | custom-call | tf_op jit(solution)/shard_map/experts/pallas_call | solution.py:505
  131.3 1.9 %copy.26 = bf16[128,2048]{1,0:T(8,128)(2,1)} copy(bf16[128,2048]{1,0:T(8,128)(2,1)} %experts.1) | data formatting | bytes 1048576
Async XLA Ops:
  4.8 0.9 copy-start.1
  5.7 0.9 copy-start.2
  6.6 0.9 copy-start.3
  7.5 0.9 copy-start.4
  8.4 0.9 copy-start.5
  9.4 0.8 copy-start.6
  10.1 0.8 copy-start.7
  10.9 0.7 copy-start.8
  11.5 0.7 copy-start.9
  55.2 0.7 copy-start

commit v4 on v3

--- a/solution.py
+++ b/solution.py
@@ -107,10 +107,45 @@
 SENDS = [(e, axis, step, target) for e in list(OWN) + EVENTS for axis, step, target in sends_of(e)]
 
 
-def attention_kernel(
-    query_ref, key_ref, value_ref, docs_ref, qgain_ref, kgain_ref, rowc_ref, rows_ref, colc_ref, cols_ref,
+GROUPS = 4
+DEVICES = NZ * NY * NC * NX
+PER_GROUP = DEVICES // GROUPS
+
+
+def exchange_order():
+    every = [(a, b, c, d) for a in range(NZ) for b in range(NY) for c in range(NC) for d in range(NX)]
+    far = lambda o: min(o[0], NZ - o[0]) + min(o[1], NY - o[1]) + min(o[3], NX - o[3])
+    others = [o for o in every if any(o)]
+    return sorted(others, key=lambda o: (-far(o), o[3], o[1], o[0], o[2])) + [(0, 0, 0, 0)]
+
+
+ORDER = exchange_order()
+
+
+def order_table():
+    table = np.zeros((1, DEVICES), np.float32)
+    for n, (dz, dy, dc, dx) in enumerate(ORDER):
+        table[0, ((dz * NY + dy) * NC + dc) * NX + dx] = n
+    return table
+
+
+def norm_rows(stream, gain, bias):
+    center = jnp.mean(stream, axis=-1, keepdims=True)
+    spread = jnp.mean(jnp.square(stream - center), axis=-1, keepdims=True)
+    return (stream - center) * lax.rsqrt(spread + eps_norm) * gain + bias
+
+
+def layer_kernel(
+    query_hbm, key_hbm, value_hbm, docs_hbm, qgain_hbm, kgain_hbm, rowc_hbm, rows_hbm, colc_hbm, cols_hbm,
+    res_hbm, routes_hbm, weights_hbm, order_hbm, ogain_hbm, mgain_hbm, mbias_hbm, fgain_hbm, fbias_hbm,
+    proj_hbm, gate_hbm, up_hbm, down_hbm,
     out_ref,
-    slots, queries, acc, top, low, send_sem, recv_sem, pair_send, pair_recv,
+    query_ref, key_ref, docs_ref, qgain_ref, kgain_ref, rowc_ref, rows_ref, colc_ref, cols_ref,
+    res_ref, routes_ref, weights_ref, order_ref, ogain_ref, mgain_ref, mbias_ref, fgain_ref, fbias_ref,
+    proj, gate, up, down,
+    slots, queries, acc, top, low, slot_columns, weight_columns, slot_rows, choose,
+    att_ref, att_buf, stream, mid, sent, got, served, back, picked, xs,
+    load_sem, send_sem, recv_sem, pair_send, pair_recv, att_send, att_recv, go_send, go_recv, ret_send, ret_recv,
 ):
     sp, tp = lax.axis_index("sp"), lax.axis_index("tp")
     core = sp % NC
@@ -119,6 +154,14 @@
     rows = key_ref.shape[0]
     half_rows = rows // 2
     heads = query_ref.shape[1] // HEAD
+    tokens, width = res_ref.shape
+    chunks = width // WIDE
+    block = CAP * chunks
+    group_rows = PER_GROUP * block
+    zs = [((z + d) % NZ) * (NY * NC) for d in range(NZ)]
+    ys = [((y + d) % NY) * NC for d in range(NY)]
+    cs = [(core + d) % NC for d in range(NC)]
+    xs_at = [(tp + d) % NX for d in range(NX)]
     partner = sp + 1 - 2 * core
     near = {}
     for step in (1, -1):
@@ -126,8 +169,34 @@
         near[False, step] = ((z + NZ + step) % NZ) * (NY * NC) + y * NC + core
 
     barrier = pltpu.get_barrier_semaphore()
-    for to in list(near.values()) + [partner]:
-        pl.semaphore_signal(barrier, inc=1, device_id=(to, tp), device_id_type=MESH)
+
+    @pl.loop(1, DEVICES)
+    def _(n):
+        to_sp = ((z + n // (NY * NC * NX)) % NZ) * (NY * NC) + ((y + n // (NC * NX)) % NY) * NC + (core + n // NX) % NC
+        pl.semaphore_signal(barrier, inc=1, device_id=(to_sp, (tp + n) % NX), device_id_type=MESH)
+
+    first = (key_hbm, docs_hbm, kgain_hbm, rowc_hbm, rows_hbm, colc_hbm, cols_hbm)
+    first_in = (key_ref, docs_ref, kgain_ref, rowc_ref, rows_ref, colc_ref, cols_ref)
+    later = (query_hbm, qgain_hbm, routes_hbm, weights_hbm, order_hbm, res_hbm, ogain_hbm, mgain_hbm, mbias_hbm, fgain_hbm, fbias_hbm)
+    later_in = (query_ref, qgain_ref, routes_ref, weights_ref, order_ref, res_ref, ogain_ref, mgain_ref, mbias_ref, fgain_ref, fbias_ref)
+    last = (proj_hbm, gate_hbm.at[0], up_hbm.at[0], down_hbm.at[0])
+    last_in = (proj, gate, up, down)
+    pairs = list(zip(first + later + last, first_in + later_in + last_in))
+    loads = [pltpu.make_async_copy(src, dst, load_sem.at[n]) for n, (src, dst) in enumerate(pairs)]
+    first_loads, later_loads, last_loads = loads[: len(first)], loads[len(first) : len(first + later)], loads[len(first + later) :]
+    value_loads = [
+        pltpu.make_async_copy(
+            value_hbm.at[pl.ds(h * half_rows + k * HEAD, HEAD), :],
+            slots.at[unit_of(OWN[h]), 0, pl.ds(HEAD + DOC_ROWS, HEAD), pl.ds(k * HEAD, HEAD)],
+            load_sem.at[len(pairs) + 2 * h + k],
+        )
+        for h in range(2)
+        for k in range(2)
+    ]
+    for load in first_loads + value_loads + later_loads + last_loads:
+        load.start()
+    for load in first_loads:
+        load.wait()
 
     def table(row_ref, col_ref):
         mine = row_ref[pl.ds(pl.multiple_of(sp * 8, 8), 8), :]
@@ -140,13 +209,11 @@
         part = slice(h * half_rows, (h + 1) * half_rows)
         unit = unit_of(OWN[h])
         slots[unit, 0, 0:HEAD, :] = jnp.transpose(turned[part, :]).astype(jnp.bfloat16)
-        same = (numbers[0:DOC_ROWS, :] == docs_ref[h : h + 1, :]).astype(jnp.float32)
+        same = (numbers[0:DOC_ROWS, :] == docs_ref[:, h * half_rows : (h + 1) * half_rows]).astype(jnp.float32)
         slots[unit, 0, HEAD : HEAD + DOC_ROWS, :] = same.astype(jnp.bfloat16)
-        for k in range(2):
-            slots[unit, 0, HEAD + DOC_ROWS :, k * HEAD : (k + 1) * HEAD] = value_ref[
-                h * half_rows + k * HEAD : h * half_rows + (k + 1) * HEAD, :
-            ]
-    pl.semaphore_wait(barrier, 5)
+    for load in value_loads:
+        load.wait()
+    pl.semaphore_wait(barrier, DEVICES - 1)
 
     def sent_copy(number):
         event, axis, step, target = SENDS[number]
@@ -180,14 +247,49 @@
 
     for event in OWN:
         pass_on(event)
-
-    columns = [jnp.transpose((numbers == docs_ref[h : h + 1, :]).astype(jnp.float32)) for h in range(2)]
+    for load in later_loads:
+        load.wait()
+
+    columns = [jnp.transpose((numbers == docs_ref[:, h * half_rows : (h + 1) * half_rows]).astype(jnp.float32)) for h in range(2)]
     same = (jnp.concatenate(columns, axis=0) * SAME_DOC).astype(jnp.bfloat16)
     for head in range(heads):
         queries[head, :, 0:HEAD] = turn(
             query_ref[:, head * HEAD : (head + 1) * HEAD].astype(jnp.float32), qgain_ref[...], cosine, sine
         )
         queries[head, :, HEAD:] = same[:, 0:DOC_ROWS]
+    lane = lax.broadcasted_iota(jnp.int32, (tokens, DEVICES), 1)
+
+    def column(row):
+        return jnp.transpose(jnp.broadcast_to(row, (DEVICES, tokens)))
+
+    named = [column(routes_ref[k : k + 1, :].astype(jnp.float32)).astype(jnp.int32) for k in (0, 1)]
+    hot = [(e == lane).astype(jnp.float32) for e in named]
+    earlier = (lax.broadcasted_iota(jnp.int32, (tokens, tokens), 1) < lax.broadcasted_iota(jnp.int32, (tokens, tokens), 0)).astype(
+        jnp.float32
+    )
+    counted = jnp.dot(
+        earlier.astype(jnp.bfloat16), (hot[0] + hot[1]).astype(jnp.bfloat16), preferred_element_type=jnp.float32
+    )
+    for k in (0, 1):
+        rank = jnp.sum(hot[k] * counted, axis=1, keepdims=True)
+        e = named[k]
+        dx = ((e & 3) + NX - tp) & 3
+        dc = (((e >> 2) & 1) + core) & 1
+        dy = (((e >> 3) & 3) + NY - y) & 3
+        dz = ((e >> 5) + NZ - z) & 3
+        relative = ((dz * NY + dy) * NC + dc) * NX + dx
+        place = jnp.sum(jnp.where(relative == lane, order_ref[...], 0.0), axis=1, keepdims=True)
+        slot = jnp.broadcast_to(place * block + rank, (tokens, DEVICES))
+        slot_columns[k] = slot.astype(jnp.int32)
+        weight_columns[k] = column(weights_ref[k : k + 1, :])
+        slot_rows[k] = jnp.transpose(slot)[0:8, :].astype(jnp.int32)
+    slot_row = [
+        jnp.concatenate([slot_rows[k, 0:1, :] + CAP * c for c in range(chunks)], axis=1) for k in (0, 1)
+    ]
+    for g in range(GROUPS):
+        at_row = lax.broadcasted_iota(jnp.int32, (group_rows, chunks * tokens), 0) + g * group_rows
+        taken = (at_row == slot_row[0]) | (at_row == slot_row[1])
+        choose[g * group_rows : (g + 1) * group_rows, :] = taken.astype(jnp.float32).astype(jnp.bfloat16)
     acc[...] = jnp.zeros_like(acc)
     low[...] = jnp.zeros_like(low)
     top[...] = jnp.full_like(top, -1e20)
@@ -235,88 +337,7 @@
     lax.fori_loop(0, len(GAPS), step, 0)
     for h in range(heads):
         total = jnp.sum(low[h], axis=1, keepdims=True)
-        out_ref[:, h * HEAD : (h + 1) * HEAD] = (acc[h] / total).astype(jnp.bfloat16)
-    for number in range(len(SENDS)):
-        sent_copy(number).wait_send()
-    for number, event in enumerate(list(OWN) + EVENTS):
-        pair_copy(event, number).wait_send()
-
-
-def norm_rows(stream, gain, bias):
-    center = jnp.mean(stream, axis=-1, keepdims=True)
-    spread = jnp.mean(jnp.square(stream - center), axis=-1, keepdims=True)
-    return (stream - center) * lax.rsqrt(spread + eps_norm) * gain + bias
-
-
-def expert_kernel(
-    att_ref, res_ref, routes_ref, weights_ref, ogain_ref, mgain_ref, mbias_ref, fgain_ref, fbias_ref,
-    proj_hbm, gate_hbm, up_hbm, down_hbm,
-    out_ref,
-    att_buf, proj, gate, up, down, stream, mid, sent, got, served, back, picked, xs,
-    load_sem, att_send, att_recv, go_send, go_recv, ret_send, ret_recv,
-):
-    sp, tp = lax.axis_index("sp"), lax.axis_index("tp")
-    core = sp % NC
-    y = (sp // NC) % NY
-    z = sp // (NC * NY)
-    tokens = res_ref.shape[0]
-    width = res_ref.shape[1]
-    chunks = width // WIDE
-    block = CAP * chunks
-    groups = 4
-    per_group = NZ * NY * NC * NX // groups
-    group_rows = per_group * block
-
-    loads = [
-        pltpu.make_async_copy(src, dst, load_sem.at[n])
-        for n, (src, dst) in enumerate(((proj_hbm, proj), (gate_hbm.at[0], gate), (up_hbm.at[0], up), (down_hbm.at[0], down)))
-    ]
-    for load in loads:
-        load.start()
-
-    def steps(g, r):
-        dx, dy, dc = r // (NY * NC), (r // NC) % NY, r % NC
-        return dx, dy, (g + 8 - dx - dy) % NZ, dc
-
-    def device_at(g, r, sign):
-        dx, dy, dz, dc = steps(g, r)
-        new_z = (z + NZ + sign * dz) % NZ
-        new_y = (y + NY + sign * dy) % NY
-        new_c = (core + dc) % NC
-        new_x = (tp + NX + sign * dx) % NX
-        return (new_z * (NY * NC) + new_y * NC + new_c, new_x)
-
-    barrier = pltpu.get_barrier_semaphore()
-    for g in range(groups):
-
-        @pl.loop(1 if g == 0 else 0, per_group)
-        def _(r, g=g):
-            pl.semaphore_signal(barrier, inc=1, device_id=device_at(g, r, 1), device_id_type=MESH)
-
-    named = routes_ref[...]
-    expert_lane = lax.broadcasted_iota(jnp.int32, (tokens, 128), 1)
-    hot = [(named[:, k : k + 1] == expert_lane).astype(jnp.float32) for k in (0, 1)]
-    earlier = (
-        lax.broadcasted_iota(jnp.int32, (tokens, tokens), 1) < lax.broadcasted_iota(jnp.int32, (tokens, tokens), 0)
-    ).astype(jnp.bfloat16)
-    counted = jnp.dot(earlier, (hot[0] + hot[1]).astype(jnp.bfloat16), preferred_element_type=jnp.float32)
-    slot_column, slot_row = [], []
-    for k in (0, 1):
-        rank = jnp.sum(hot[k] * counted, axis=1, keepdims=True).astype(jnp.int32)
-        e = named[:, k : k + 1]
-        dx = ((e & 3) + NX - tp) & 3
-        dc = (((e >> 2) & 1) + core) & 1
-        dy = (((e >> 3) & 3) + NY - y) & 3
-        dz = ((e >> 5) + NZ - z) & 3
-        place = ((dx + dy + dz) & 3) * per_group + dx * (NY * NC) + dy * NC + dc
-        column = place * block + rank
-        slot_column.append(column)
-        turned = jnp.transpose(jnp.broadcast_to(column.astype(jnp.float32), (tokens, 128)))
-        row = turned[0:1, :].astype(jnp.int32)
-        slot_row.append(jnp.concatenate([row + CAP * c for c in range(chunks)], axis=1))
-
-    pl.semaphore_wait(barrier, NZ * NY * NC * NX - 1)
-
+        att_ref[:, h * HEAD : (h + 1) * HEAD] = (acc[h] / total).astype(jnp.bfloat16)
     copies = []
     for j in range(1, NX):
         to = (tp + j) % NX
@@ -331,7 +352,7 @@
         copy.start()
         copies.append(copy)
 
-    loads[0].wait()
+    last_loads[0].wait()
     squares = jnp.zeros((tokens, 1), jnp.float32)
     local = att_ref.shape[1]
     for j in range(NX):
@@ -343,7 +364,8 @@
             part = att_buf[j]
         part = part.astype(jnp.float32)
         squares = squares + jnp.sum(part * part, axis=1, keepdims=True)
-        scaled = (part * ogain_ref[pl.ds(source, 1), :]).astype(jnp.bfloat16)
+        gain = ogain_ref[:, pl.ds(pl.multiple_of(source * local, local), local)]
+        scaled = (part * gain).astype(jnp.bfloat16)
         product = jnp.dot(
             scaled, proj[pl.ds(pl.multiple_of(source * local, local), local), :], preferred_element_type=jnp.float32
         )
@@ -361,35 +383,34 @@
         for c in range(chunks):
             mid[c * tokens + n * step_rows : c * tokens + (n + 1) * step_rows, :] = value[:, c * WIDE : (c + 1) * WIDE]
 
-    def row_iota(g):
-        return lax.broadcasted_iota(jnp.int32, (group_rows, chunks * tokens), 0) + g * group_rows
-
-    for g in range(groups):
-        rows = row_iota(g)
-        choose = ((rows == slot_row[0]) | (rows == slot_row[1])).astype(jnp.float32).astype(jnp.bfloat16)
-        sent[g * group_rows : (g + 1) * group_rows, :] = jnp.dot(
-            choose, mid[...], preferred_element_type=jnp.float32
-        ).astype(jnp.bfloat16)
-
-        @pl.loop(1 if g == 0 else 0, per_group)
-        def _(r, g=g):
-            at = pl.ds(pl.multiple_of((g * per_group + r) * block, block), block)
+    def exchange(g, source, target, sends, receives, sign):
+        for n in range(g * PER_GROUP, (g + 1) * PER_GROUP):
+            dz, dy, dc, dx = ORDER[n]
+            if not any(ORDER[n]):
+                continue
+            at = pl.ds(n * block, block)
             pltpu.make_async_remote_copy(
-                src_ref=sent.at[at, :],
-                dst_ref=got.at[at, :],
-                send_sem=go_send.at[g],
-                recv_sem=go_recv.at[g],
-                device_id=device_at(g, r, 1),
+                src_ref=source.at[at, :],
+                dst_ref=target.at[at, :],
+                send_sem=sends.at[g],
+                recv_sem=receives.at[g],
+                device_id=(zs[sign * dz % NZ] + ys[sign * dy % NY] + cs[dc], xs_at[sign * dx % NX]),
                 device_id_type=MESH,
             ).start()
 
-    got[0:block, :] = sent[0:block, :]
-    for load in loads[1:]:
+    for g in range(GROUPS):
+        sent[g * group_rows : (g + 1) * group_rows, :] = jnp.dot(
+            choose[g * group_rows : (g + 1) * group_rows, :], mid[...], preferred_element_type=jnp.float32
+        ).astype(jnp.bfloat16)
+        exchange(g, sent, got, go_send, go_recv, 1)
+
+    own_block = slice((DEVICES - 1) * block, DEVICES * block)
+    got[own_block, :] = sent[own_block, :]
+    for load in last_loads[1:]:
         load.wait()
 
     def whole(ref, g):
-        first = block if g == 0 else 0
-        return ref.at[pl.ds(g * group_rows + first, group_rows - first), :]
+        return ref.at[pl.ds(g * group_rows, group_rows - (block if g == GROUPS - 1 else 0)), :]
 
     sub = 256
     ii = lax.broadcasted_iota(jnp.int32, (sub, sub), 0)
@@ -401,7 +422,7 @@
 
     collect = (jj == spot(ii)).astype(jnp.float32).astype(jnp.bfloat16)
     scatter = (ii == spot(jj)).astype(jnp.float32).astype(jnp.bfloat16)
-    for g in range(groups):
+    for g in range(GROUPS):
         pltpu.make_async_copy(whole(got, g), whole(got, g), go_recv.at[g]).wait()
         for s in range(group_rows // sub):
             ordered = jnp.dot(
@@ -424,29 +445,19 @@
                 scatter, stacked, preferred_element_type=jnp.float32
             ).astype(jnp.bfloat16)
 
-        @pl.loop(1 if g == 0 else 0, per_group)
-        def _(r, g=g):
-            at = pl.ds(pl.multiple_of((g * per_group + r) * block, block), block)
-            pltpu.make_async_remote_copy(
-                src_ref=served.at[at, :],
-                dst_ref=back.at[at, :],
-                send_sem=ret_send.at[g],
-                recv_sem=ret_recv.at[g],
-                device_id=device_at(g, r, -1),
-                device_id_type=MESH,
-            ).start()
-
-    back[0:block, :] = served[0:block, :]
-
-    for g in range(groups):
+        exchange(g, served, back, ret_send, ret_recv, -1)
+
+    back[own_block, :] = served[own_block, :]
+
+    for g in range(GROUPS):
         pltpu.make_async_copy(whole(back, g), whole(back, g), ret_recv.at[g]).wait()
         lanes = lax.broadcasted_iota(jnp.int32, (tokens, group_rows), 1) + g * group_rows
         arrived = back[g * group_rows : (g + 1) * group_rows, :]
         for c in range(chunks):
             total = jnp.zeros((tokens, WIDE), jnp.float32)
             for k in (0, 1):
-                choose = (lanes == slot_column[k] + CAP * c).astype(jnp.float32).astype(jnp.bfloat16)
-                total = total + weights_ref[:, k : k + 1] * jnp.dot(choose, arrived, preferred_element_type=jnp.float32)
+                mine = (lanes == slot_columns[k, :, 0:1] + CAP * c).astype(jnp.float32).astype(jnp.bfloat16)
+                total = total + weight_columns[k, :, 0:1] * jnp.dot(mine, arrived, preferred_element_type=jnp.float32)
             if g == 0:
                 picked[:, c * WIDE : (c + 1) * WIDE] = total
             else:
@@ -462,9 +473,13 @@
 
     for copy in copies:
         copy.wait_send()
-    for g in range(groups):
+    for g in range(GROUPS):
         pltpu.make_async_copy(whole(sent, g), whole(sent, g), go_send.at[g]).wait()
         pltpu.make_async_copy(whole(served, g), whole(served, g), ret_send.at[g]).wait()
+    for number in range(len(SENDS)):
+        sent_copy(number).wait_send()
+    for number, event in enumerate(list(OWN) + EVENTS):
+        pair_copy(event, number).wait_send()
 
 
 def per_device(
@@ -473,70 +488,62 @@
 ):
     rows = queries.shape[0]
     heads = queries.shape[1] // HEAD
-    docs = documents.reshape(2, rows // 2)
-    attention = pl.pallas_call(
-        attention_kernel,
-        out_shape=jax.ShapeDtypeStruct((rows, heads * HEAD), jnp.bfloat16),
-        in_specs=[VMEM] * 10,
+    tokens, width = residual.shape
+    chunks = width // WIDE
+    slots = DEVICES * CAP * chunks
+    vec = lambda v: v.reshape(1, -1)
+    tables = [jnp.asarray(t) for t in table_constants()]
+    inputs = (
+        queries, key_heads, value_heads, vec(documents), vec(query_gain), vec(key_gain), *tables,
+        residual, routes.T, route_weights.T, jnp.asarray(order_table()), vec(out_gain), vec(mid_gain), vec(mid_bias),
+        vec(final_gain), vec(final_bias), out_proj, expert_gate, expert_up, expert_down,
+    )
+    held = [v for n, v in enumerate(inputs) if n != 2]
+    f32, bf16, i32 = jnp.float32, jnp.bfloat16, jnp.int32
+    dma = pltpu.SemaphoreType.DMA
+    return pl.pallas_call(
+        layer_kernel,
+        out_shape=jax.ShapeDtypeStruct((tokens, width), bf16),
+        in_specs=[ANY] * len(inputs),
         out_specs=VMEM,
-        scratch_shapes=[
-            pltpu.VMEM((len(UNITS), NC, HALF_ROWS, 2 * HEAD), jnp.bfloat16),
-            pltpu.VMEM((heads, rows, HEAD + DOC_ROWS), jnp.bfloat16),
-            pltpu.VMEM((heads, rows, HEAD), jnp.float32),
-            pltpu.VMEM((heads, rows, HEAD), jnp.float32),
-            pltpu.VMEM((heads, rows, HEAD), jnp.float32),
-            pltpu.SemaphoreType.DMA((len(SENDS),)),
-            pltpu.SemaphoreType.DMA((len(EVENTS),)),
-            pltpu.SemaphoreType.DMA((len(EVENTS) + 2,)),
-            pltpu.SemaphoreType.DMA((len(UNITS),)),
+        scratch_shapes=[pltpu.VMEM(v.shape[-2:], v.dtype) for v in held]
+        + [
+            pltpu.VMEM((len(UNITS), NC, HALF_ROWS, 2 * HEAD), bf16),
+            pltpu.VMEM((heads, rows, HEAD + DOC_ROWS), bf16),
+            pltpu.VMEM((heads, rows, HEAD), f32),
+            pltpu.VMEM((heads, rows, HEAD), f32),
+            pltpu.VMEM((heads, rows, HEAD), f32),
+            pltpu.VMEM((2, tokens, DEVICES), i32),
+            pltpu.VMEM((2, tokens, DEVICES), f32),
+            pltpu.VMEM((2, 8, tokens), i32),
+            pltpu.VMEM((slots, chunks * tokens), bf16),
+            pltpu.VMEM((rows, heads * HEAD), bf16),
+            pltpu.VMEM((NX, tokens, heads * HEAD), bf16),
+            pltpu.VMEM((tokens, width), f32),
+            pltpu.VMEM((chunks * tokens, WIDE), bf16),
+            pltpu.VMEM((slots, WIDE), bf16),
+            pltpu.VMEM((slots, WIDE), bf16),
+            pltpu.VMEM((slots, WIDE), bf16),
+            pltpu.VMEM((slots, WIDE), bf16),
+            pltpu.VMEM((tokens, width), f32),
+            pltpu.VMEM((tokens, width), bf16),
+            dma((len(inputs) + 3,)),
+            dma((len(SENDS),)),
+            dma((len(EVENTS),)),
+            dma((len(EVENTS) + 2,)),
+            dma((len(UNITS),)),
+            dma((NX,)),
+            dma((NX,)),
+            dma((GROUPS,)),
+            dma((GROUPS,)),
+            dma((GROUPS,)),
+            dma((GROUPS,)),
         ],
         compiler_params=pltpu.CompilerParams(
-            collective_id=0, has_side_effects=True, vmem_limit_bytes=48 * 1024 * 1024
+            collective_id=0, has_side_effects=True, vmem_limit_bytes=60 * 1024 * 1024
         ),
-        name="attention",
-    )(
-        queries, key_heads, value_heads, docs, query_gain.reshape(1, HEAD), key_gain.reshape(1, HEAD),
-        *[jnp.asarray(t) for t in table_constants()],
-    )
-    tokens, width = residual.shape
-    hidden = expert_gate.shape[2]
-    slots = NZ * NY * NC * NX * CAP * (width // WIDE)
-    vec = lambda v: v.reshape(1, -1)
-    return pl.pallas_call(
-        expert_kernel,
-        out_shape=jax.ShapeDtypeStruct((tokens, width), jnp.bfloat16),
-        in_specs=[VMEM] * 9 + [ANY] * 4,
-        out_specs=VMEM,
-        scratch_shapes=[
-            pltpu.VMEM((NX, tokens, heads * HEAD), jnp.bfloat16),
-            pltpu.VMEM(out_proj.shape, jnp.bfloat16),
-            pltpu.VMEM((width, hidden), jnp.bfloat16),
-            pltpu.VMEM((width, hidden), jnp.bfloat16),
-            pltpu.VMEM((hidden, width), jnp.bfloat16),
-            pltpu.VMEM((tokens, width), jnp.float32),
-            pltpu.VMEM((width // WIDE * tokens, WIDE), jnp.bfloat16),
-            pltpu.VMEM((slots, WIDE), jnp.bfloat16),
-            pltpu.VMEM((slots, WIDE), jnp.bfloat16),
-            pltpu.VMEM((slots, WIDE), jnp.bfloat16),
-            pltpu.VMEM((slots, WIDE), jnp.bfloat16),
-            pltpu.VMEM((tokens, width), jnp.float32),
-            pltpu.VMEM((tokens, width), jnp.bfloat16),
-            pltpu.SemaphoreType.DMA((4,)),
-            pltpu.SemaphoreType.DMA((NX,)),
-            pltpu.SemaphoreType.DMA((NX,)),
-            pltpu.SemaphoreType.DMA((4,)),
-            pltpu.SemaphoreType.DMA((4,)),
-            pltpu.SemaphoreType.DMA((4,)),
-            pltpu.SemaphoreType.DMA((4,)),
-        ],
-        compiler_params=pltpu.CompilerParams(
-            collective_id=1, has_side_effects=True, vmem_limit_bytes=56 * 1024 * 1024
-        ),
-        name="experts",
-    )(
-        attention, residual, routes, route_weights, out_gain.reshape(NX, -1), vec(mid_gain), vec(mid_bias),
-        vec(final_gain), vec(final_bias), out_proj, expert_gate, expert_up, expert_down,
-    )
+        name="layer",
+    )(*inputs)
 
 
 def solution(mesh):

time: 134 us -> 122 us (0.910)
  local copies, waits for them, and re-layouts: 14.7 us -> 1.88 us
    unnamed x23 -> x1, local copies, waits for them, and re-layouts: 12.8 us -> 1.88 us
    reshape x2 -> x0, local copies, waits for them, and re-layouts: 1.98 us -> none  [the longest x1 1.28 us: per_device(): out_gain.reshape(NX, -1)]
    pallas_call x2 -> x1, Pallas kernels: 118 us -> 119 us  [per_device(): pl.pallas_call(layer_kernel, out_shape=jax.ShapeDtypeStruct((tokens, widt...]
where the time goes in v4:
time: 122 us; the launch traced here: 121 us
  Pallas kernels  119 us (98%)
  local copies, waits for them, and re-layouts  1.88 us (2%)
    pallas_call x1, Pallas kernels, per_device(): pl.pallas_call(layer_kernel, out_shape=jax.ShapeDtypeStruct((tokens, widt...  119 us

profile of v4, /device:TPU:1, one launch (start us, length us, event | category | flops | bytes accessed | tf_op | source)
XLA Modules:
  0.0 120.7 jit_solution(12428119181588966391)
XLA Ops:
  0.0 118.8 %layer.1 = bf16[128,2048]{1,0:T(8,128)(2,1)} custom-call(bf16[512,256]{1,0:T(8,128)(2,1)} %query_hbm.1, bf16[512,128]{1,0:T(8,128)(2,1)} %key_hbm.1, bf16[512,128]{1,0:T(8,128)(2,1)} %value_hbm.1, s32[1,512]{1,0:T(1,128)} %bitcast.15, f32[1,128]{1,0:T(1,128)} %bitcast.18, f32[1,128]{1,0:T(1,128)} %bitcast.19, f32[256,128]{1,0:T(8,128)} %constant.10.clone.rowc_hbm, ...), custom_call_target="tpu_custom_call" | custom-call | tf_op jit(solution)/shard_map/layer/pallas_call | solution.py:504
  118.8 1.9 %copy.25 = bf16[128,2048]{1,0:T(8,128)(2,1)} copy(bf16[128,2048]{1,0:T(8,128)(2,1)} %layer.1) | data formatting | bytes 1048576

commit v5 on v4

--- a/solution.py
+++ b/solution.py
@@ -116,7 +116,7 @@
     every = [(a, b, c, d) for a in range(NZ) for b in range(NY) for c in range(NC) for d in range(NX)]
     far = lambda o: min(o[0], NZ - o[0]) + min(o[1], NY - o[1]) + min(o[3], NX - o[3])
     others = [o for o in every if any(o)]
-    return sorted(others, key=lambda o: (-far(o), o[3], o[1], o[0], o[2])) + [(0, 0, 0, 0)]
+    return sorted(others, key=lambda o: ((sum(o) - o[2]) % GROUPS, -far(o), o)) + [(0, 0, 0, 0)]
 
 
 ORDER = exchange_order()
@@ -170,10 +170,10 @@
 
     barrier = pltpu.get_barrier_semaphore()
 
-    @pl.loop(1, DEVICES)
-    def _(n):
-        to_sp = ((z + n // (NY * NC * NX)) % NZ) * (NY * NC) + ((y + n // (NC * NX)) % NY) * NC + (core + n // NX) % NC
-        pl.semaphore_signal(barrier, inc=1, device_id=(to_sp, (tp + n) % NX), device_id_type=MESH)
+    for to in list(near.values()) + [partner]:
+        pl.semaphore_signal(barrier, inc=1, device_id=(to, tp), device_id_type=MESH)
+    for to in xs_at[1:]:
+        pl.semaphore_signal(barrier, inc=1, device_id=(sp, to), device_id_type=MESH)
 
     first = (key_hbm, docs_hbm, kgain_hbm, rowc_hbm, rows_hbm, colc_hbm, cols_hbm)
     first_in = (key_ref, docs_ref, kgain_ref, rowc_ref, rows_ref, colc_ref, cols_ref)
@@ -213,7 +213,7 @@
         slots[unit, 0, HEAD : HEAD + DOC_ROWS, :] = same.astype(jnp.bfloat16)
     for load in value_loads:
         load.wait()
-    pl.semaphore_wait(barrier, DEVICES - 1)
+    pl.semaphore_wait(barrier, 5 + NX - 1)
 
     def sent_copy(number):
         event, axis, step, target = SENDS[number]

time: 122 us -> 105 us (0.86)
  Pallas kernels: 119 us -> 103 us
    pallas_call x1, Pallas kernels: 119 us -> 103 us  [per_device(): pl.pallas_call(layer_kernel, out_shape=jax.ShapeDtypeStruct((tokens, widt...]
where the time goes in v5:
time: 105 us
  Pallas kernels  103 us (98%)
  local copies, waits for them, and re-layouts  1.88 us (2%)
    pallas_call x1, Pallas kernels, per_device(): pl.pallas_call(layer_kernel, out_shape=jax.ShapeDtypeStruct((tokens, widt...  103 us

profile of v5, /device:TPU:1, one launch (start us, length us, event | category | flops | bytes accessed | tf_op | source)
XLA Modules:
  0.0 104.6 jit_solution(7957192618774724686)
XLA Ops:
  0.0 102.7 %layer.1 = bf16[128,2048]{1,0:T(8,128)(2,1)} custom-call(bf16[512,256]{1,0:T(8,128)(2,1)} %query_hbm.1, bf16[512,128]{1,0:T(8,128)(2,1)} %key_hbm.1, bf16[512,128]{1,0:T(8,128)(2,1)} %value_hbm.1, s32[1,512]{1,0:T(1,128)} %bitcast.15, f32[1,128]{1,0:T(1,128)} %bitcast.18, f32[1,128]{1,0:T(1,128)} %bitcast.19, f32[256,128]{1,0:T(8,128)} %constant.10.clone.rowc_hbm, ...), custom_call_target="tpu_custom_call" | custom-call | tf_op jit(solution)/shard_map/layer/pallas_call | solution.py:504
  102.7 1.9 %copy.25 = bf16[128,2048]{1,0:T(8,128)(2,1)} copy(bf16[128,2048]{1,0:T(8,128)(2,1)} %layer.1) | data formatting | bytes 1048576

commit v6 on v5

--- a/solution.py
+++ b/solution.py
@@ -107,7 +107,7 @@
 SENDS = [(e, axis, step, target) for e in list(OWN) + EVENTS for axis, step, target in sends_of(e)]
 
 
-GROUPS = 4
+GROUPS = 8
 DEVICES = NZ * NY * NC * NX
 PER_GROUP = DEVICES // GROUPS
 
@@ -116,7 +116,7 @@
     every = [(a, b, c, d) for a in range(NZ) for b in range(NY) for c in range(NC) for d in range(NX)]
     far = lambda o: min(o[0], NZ - o[0]) + min(o[1], NY - o[1]) + min(o[3], NX - o[3])
     others = [o for o in every if any(o)]
-    return sorted(others, key=lambda o: ((sum(o) - o[2]) % GROUPS, -far(o), o)) + [(0, 0, 0, 0)]
+    return sorted(others, key=lambda o: ((sum(o) - o[2]) % 4, o[2], -far(o), o)) + [(0, 0, 0, 0)]
 
 
 ORDER = exchange_order()
@@ -432,7 +432,7 @@
                 xs[s * per_chunk : (s + 1) * per_chunk, c * WIDE : (c + 1) * WIDE] = ordered[
                     c * per_chunk : (c + 1) * per_chunk, :
                 ]
-        x = xs[...]
+        x = xs[0 : PER_GROUP * CAP, :]
         gate_part = jnp.dot(x, gate[...], preferred_element_type=jnp.float32)
         up_part = jnp.dot(x, up[...], preferred_element_type=jnp.float32)
         hidden = (gate_part / (1.0 + jnp.exp(-gate_part)) * up_part).astype(jnp.bfloat16)

time: 105 us -> 104 us (level)
  no operation moved by 1% of the time
where the time goes in v6:
time: 104 us
  Pallas kernels  102 us (98%)
  local copies, waits for them, and re-layouts  1.88 us (2%)
    pallas_call x1, Pallas kernels, per_device(): pl.pallas_call(layer_kernel, out_shape=jax.ShapeDtypeStruct((tokens, widt...  102 us

profile of v6, /device:TPU:1, one launch (start us, length us, event | category | flops | bytes accessed | tf_op | source)
XLA Modules:
  0.0 104.2 jit_solution(1464932104236416726)
XLA Ops:
  0.0 102.3 %layer.1 = bf16[128,2048]{1,0:T(8,128)(2,1)} custom-call(bf16[512,256]{1,0:T(8,128)(2,1)} %query_hbm.1, bf16[512,128]{1,0:T(8,128)(2,1)} %key_hbm.1, bf16[512,128]{1,0:T(8,128)(2,1)} %value_hbm.1, s32[1,512]{1,0:T(1,128)} %bitcast.15, f32[1,128]{1,0:T(1,128)} %bitcast.18, f32[1,128]{1,0:T(1,128)} %bitcast.19, f32[256,128]{1,0:T(8,128)} %constant.10.clone.rowc_hbm, ...), custom_call_target="tpu_custom_call" | custom-call | tf_op jit(solution)/shard_map/layer/pallas_call | solution.py:504
  102.3 1.9 %copy.25 = bf16[128,2048]{1,0:T(8,128)(2,1)} copy(bf16[128,2048]{1,0:T(8,128)(2,1)} %layer.1) | data formatting | bytes 1048576
